TPU v7x, 32 devices: a whole 2x2x4 slice. The times are simulated.
32 devices in a mesh: sp: 16 (over z, y, x), tp: 2 (over core).
Axes of the slice: x: 2, y: 2, z: 4, core: 2. Of those that a mesh axis runs over, the one named last changes fastest.
Arguments:
- mid_rows: bfloat16 [2048, 2048], P(('sp', 'tp')), may hold values from -6 to 6
- cotangent: bfloat16 [2048, 2048], P(('sp', 'tp')), may hold values from -6 to 6
- route_experts: int32 [2048, 2], P(('sp', 'tp')), may hold values from 0 to 15, as said below
- route_weights: float32 [2048, 2], P(('sp', 'tp')), may hold values from 0.05 to 0.6
- gate_weight: bfloat16 [16, 2048, 1024], P('sp', None, 'tp'), may hold values from -0.125 to 0.125
- up_weight: bfloat16 [16, 2048, 1024], P('sp', None, 'tp'), may hold values from -0.125 to 0.125
- down_weight: bfloat16 [16, 1024, 2048], P('sp', 'tp'), may hold values from -0.1875 to 0.1875
- out_weight: bfloat16 [2048, 2048], P(None, 'tp'), may hold values from -0.125 to 0.125
- queries: bfloat16 [2048, 1024], P('sp', 'tp'), may hold values from -6 to 6
- key_rows: bfloat16 [2048, 1024], P('sp', 'tp'), may hold values from -6 to 6
- value_rows: bfloat16 [2048, 2048], P('sp', 'tp'), may hold values from -6 to 6
- log_decay: float32 [2048, 1024], P('sp', 'tp'), may hold values from -1 to 0
Outputs:
- gate_gradient: bfloat16 [16, 2048, 1024], P('sp', None, 'tp')
- up_gradient: bfloat16 [16, 2048, 1024], P('sp', None, 'tp')
- down_gradient: bfloat16 [16, 1024, 2048], P('sp', 'tp')
- out_gradient: float32 [2048, 2048], P('sp', 'tp')
- query_gradient: bfloat16 [2048, 1024], P('sp', 'tp')
- key_gradient: bfloat16 [2048, 1024], P('sp', 'tp')
- value_gradient: bfloat16 [2048, 2048], P('sp', 'tp')
- decay_gradient: float32 [2048, 1024], P('sp', 'tp')
Inputs may be any that keep to these rules, and one draw needn't show every extreme that they name: `route_experts`: each row names two different experts of one group: both lie among the same 4 consecutive numbers starting at a multiple of 4. Among the rows of one device, no expert is named more than 16 times, and one expert exactly 16 times.
All inputs are finite; a program needn't handle non-finite values.
Results may differ from a plain program's by a relative error of at most 0.0058.
Values may be sent and summed in bfloat16 or wider, within the bound.
A program may use at most 192 MiB of HBM per device.

v0:
```python
import functools

import jax
import jax.numpy as jnp
from jax import lax
from jax.experimental import pallas as pl
from jax.experimental.pallas import tpu as pltpu
from jax.sharding import PartitionSpec as P

DK = 128
DV = 256
BLOCK = 64


MESH = pl.DeviceIdType.MESH
STATE = jnp.bfloat16
precise = lax.Precision.HIGH
epsilon = 1e-06
contract_rows = (((0,), (0,)), ((), ()))
contract_cols = (((1,), (1,)), ((), ()))


def others(axis, act):
    count, mine = (lax.axis_size(axis), lax.axis_index(axis))

    def turn(step, carry):
        act(step, lax.rem(mine + step, count), lax.rem(mine + count - step, count))
        return carry

    lax.fori_loop(1, count, turn, 0)


def greet(pair):
    barrier = pltpu.get_barrier_semaphore()
    total = lax.axis_size("sp") - 1
    others(
        "sp",
        lambda step, ahead, behind: pl.semaphore_signal(
            barrier, inc=1, device_id={"sp": ahead}, device_id_type=MESH
        ),
    )
    if pair:
        pl.semaphore_signal(
            barrier, inc=1, device_id={"tp": 1 - lax.axis_index("tp")}, device_id_type=MESH
        )
        total = total + 1
    pl.semaphore_wait(barrier, total)


def send(source, target, send_sem, recv_sem, where):
    return pltpu.make_async_remote_copy(
        src_ref=source,
        dst_ref=target,
        send_sem=send_sem,
        recv_sem=recv_sem,
        device_id=where,
        device_id_type=MESH,
    )


def exchange_kernel(number, pair, *refs):
    sources, targets = (refs[:number], refs[number : 2 * number])
    local_sem, send_sem, recv_sem, pass_sem, land_sem = refs[2 * number :]
    mine, core = (lax.axis_index("sp"), lax.axis_index("tp"))
    greet(pair)

    def spot(target, index, side):
        return target.at[index, side] if pair else target.at[index]

    def out(n, step, ahead, behind):
        return send(
            sources[n].at[ahead],
            spot(targets[n], mine, core),
            send_sem.at[n, step],
            recv_sem.at[n, step],
            {"sp": ahead},
        )

    def back(n, step, ahead, behind):
        return send(
            sources[n].at[ahead],
            spot(targets[n], behind, core),
            send_sem.at[n, step],
            recv_sem.at[n, step],
            {"sp": ahead},
        )

    def forward(n, step, source, index, side):
        return send(
            source,
            spot(targets[n], index, side),
            pass_sem.at[n, step],
            land_sem.at[n, step],
            {"tp": 1 - core},
        )

    for n in range(number):
        others("sp", lambda *at: out(n, *at).start())
    for n in range(number):
        pltpu.make_async_copy(
            sources[n].at[mine], spot(targets[n], mine, core), local_sem.at[n]
        ).start()
        if pair:
            forward(n, 0, sources[n].at[mine], mine, core).start()
    for n in range(number):

        def arrive(step, ahead, behind):
            back(n, step, ahead, behind).wait_recv()
            if pair:
                forward(n, step, spot(targets[n], behind, core), behind, core).start()

        others("sp", arrive)
    for n in range(number):
        others("sp", lambda *at: out(n, *at).wait_send())
        pltpu.make_async_copy(
            sources[n].at[mine], spot(targets[n], mine, core), local_sem.at[n]
        ).wait()
        if pair:

            def settle(step, ahead, behind):
                forward(n, step, spot(targets[n], behind, core), behind, core).wait_send()
                forward(n, step, spot(targets[n], behind, 1 - core), behind, 1 - core).wait_recv()

            forward(n, 0, sources[n].at[mine], mine, core).wait_send()
            forward(n, 0, sources[n].at[mine], mine, 1 - core).wait_recv()
            others("sp", settle)


def exchange(values, pair, number):
    count = lax.axis_size("sp")
    shapes = [
        jax.ShapeDtypeStruct(
            (count, 2) + part.shape[1:] if pair else part.shape, part.dtype
        )
        for part in values
    ]
    dma = pltpu.SemaphoreType.DMA
    total = len(values)
    return pl.pallas_call(
        functools.partial(exchange_kernel, total, pair),
        out_shape=shapes,
        in_specs=[pl.BlockSpec(memory_space=pltpu.VMEM)] * total,
        out_specs=[pl.BlockSpec(memory_space=pltpu.VMEM)] * total,
        scratch_shapes=[
            dma((total,)),
            dma((total, count)),
            dma((total, count)),
            dma((total, count)),
            dma((total, count)),
        ],
        compiler_params=pltpu.CompilerParams(collective_id=number, has_side_effects=True),
        name=f"exchange_{number}",
    )(*values)


def prefix_kernel(backward, total_ref, decay_ref, out_ref, got, ready, *sems):
    send_sem, recv_sem, send_two, recv_two = sems
    count, mine = (lax.axis_size("sp"), lax.axis_index("sp"))
    greet(False)

    def first(step, ahead, place):
        return send(
            total_ref.at[ahead],
            got.at[place],
            send_sem.at[step],
            recv_sem.at[step],
            {"sp": ahead},
        )

    def second(step, ahead, place):
        return send(
            ready.at[ahead],
            out_ref.at[place],
            send_two.at[step],
            recv_two.at[step],
            {"sp": ahead},
        )

    others("sp", lambda step, ahead, behind: first(step, ahead, mine).start())
    got[mine] = total_ref[mine]
    others("sp", lambda step, ahead, behind: first(step, ahead, behind).wait_recv())

    def turn(position, carry):
        index = count - 1 - position if backward else position
        ready[index] = carry.astype(ready.dtype)
        return carry * decay_ref[index][:, :1] + got[index].astype(jnp.float32)

    lax.fori_loop(0, count, turn, jnp.zeros(got.shape[1:], jnp.float32))
    others("sp", lambda step, ahead, behind: second(step, ahead, mine).start())
    out_ref[mine] = ready[mine]

    def finish(step, ahead, behind):
        first(step, ahead, mine).wait_send()
        second(step, ahead, behind).wait()

    others("sp", finish)


def prefix(total, decays, backward, number):
    count = lax.axis_size("sp")
    shape = total.shape
    pieces = total.astype(STATE).reshape(count, -1, shape[-1])
    dma = pltpu.SemaphoreType.DMA((count,))
    result = pl.pallas_call(
        functools.partial(prefix_kernel, backward),
        out_shape=jax.ShapeDtypeStruct(pieces.shape, STATE),
        in_specs=[pl.BlockSpec(memory_space=pltpu.VMEM)] * 2,
        out_specs=pl.BlockSpec(memory_space=pltpu.VMEM),
        scratch_shapes=[
            pltpu.VMEM(pieces.shape, STATE),
            pltpu.VMEM(pieces.shape, STATE),
            dma,
            dma,
            dma,
            dma,
        ],
        compiler_params=pltpu.CompilerParams(collective_id=number, has_side_effects=True),
        name=f"prefix_{number}",
    )(pieces, decays)
    return result.astype(jnp.float32).reshape(shape)


def silu_parts(pre_gate):
    gate_sigmoid = jax.nn.sigmoid(pre_gate)
    gate_swish = pre_gate * gate_sigmoid
    gate_slope = gate_sigmoid * (1.0 + pre_gate * (1.0 - gate_sigmoid))
    return (gate_swish, gate_slope)


def expert_work(rows_in, scaled, gate_local, up_local, down_local):
    pre_gate = jnp.dot(rows_in, gate_local, preferred_element_type=jnp.float32)
    pre_up = jnp.dot(rows_in, up_local, preferred_element_type=jnp.float32)
    gate_swish, gate_slope = silu_parts(pre_gate)
    hidden = (gate_swish * pre_up).astype(jnp.bfloat16)
    back_hidden = lax.dot_general(
        scaled, down_local, contract_cols, preferred_element_type=jnp.float32
    )
    back_gate = (back_hidden * pre_up * gate_slope).astype(jnp.bfloat16)
    back_up = (back_hidden * gate_swish).astype(jnp.bfloat16)
    gate_total = lax.dot_general(
        rows_in, back_gate, contract_rows, preferred_element_type=jnp.float32
    )
    up_total = lax.dot_general(rows_in, back_up, contract_rows, preferred_element_type=jnp.float32)
    down_total = lax.dot_general(hidden, scaled, contract_rows, preferred_element_type=jnp.float32)
    partial_value = lax.dot_general(
        back_gate, gate_local, contract_cols, preferred_element_type=jnp.float32
    )
    partial_value = partial_value + lax.dot_general(
        back_up, up_local, contract_cols, preferred_element_type=jnp.float32
    )
    totals = (
        gate_total.astype(jnp.bfloat16)[None],
        up_total.astype(jnp.bfloat16)[None],
        down_total.astype(jnp.bfloat16)[None],
    )
    return (totals, partial_value)


def advance(carry_state, inputs):
    factor, addend = inputs
    return (factor[:, :, None] * carry_state + addend, carry_state)


def body(
    mid_rows,
    cotangent,
    route_experts,
    route_weights,
    gate_weight,
    up_weight,
    down_weight,
    out_weight,
    queries,
    key_rows,
    value_rows,
    log_decay,
):
    experts = lax.axis_size("sp")
    row_count = route_experts.shape[0]
    capacity = 4 * row_count // experts
    model_width = mid_rows.shape[1]
    flat_expert = route_experts.reshape(-1)
    pick_order = jnp.arange(2 * row_count, dtype=jnp.int32)
    earlier = (flat_expert[None, :] == flat_expert[:, None]) & (
        pick_order[None, :] < pick_order[:, None]
    )
    slot_rank = jnp.sum(earlier.astype(jnp.int32), axis=1)
    slot_index = (flat_expert * capacity + slot_rank).reshape(row_count, 2)
    slots = jnp.arange(experts * capacity, dtype=jnp.int32)
    first_pick = slots[:, None] == slot_index[None, :, 0]
    second_pick = slots[:, None] == slot_index[None, :, 1]
    either = (first_pick | second_pick).astype(jnp.bfloat16)
    slot_weight = jnp.sum(
        jnp.where(first_pick, route_weights[None, :, 0], 0.0)
        + jnp.where(second_pick, route_weights[None, :, 1], 0.0),
        axis=1,
    )
    row_send = jnp.dot(either, mid_rows, preferred_element_type=jnp.bfloat16).reshape(
        experts, capacity, model_width
    )
    scaled_send = (
        slot_weight[:, None] * jnp.dot(either, cotangent, preferred_element_type=jnp.float32)
    ).astype(jnp.bfloat16).reshape(experts, capacity, model_width)
    local_tokens = queries.shape[0]
    heads_local = queries.shape[1] // DK
    block_count = local_tokens // BLOCK
    query_scaled = queries.astype(jnp.float32).reshape(
        block_count, BLOCK, heads_local, DK
    ) * DK ** (-0.5)
    key_float = key_rows.astype(jnp.float32).reshape(block_count, BLOCK, heads_local, DK)
    value_float = value_rows.astype(jnp.float32).reshape(block_count, BLOCK, heads_local, DV)
    decay_float = log_decay.reshape(block_count, BLOCK, heads_local, DK)
    running_log = jnp.cumsum(decay_float, axis=1)
    block_log = running_log[:, -1]
    query_decayed = query_scaled * jnp.exp(running_log)
    key_inverse = key_float * jnp.exp(-running_log)
    end_factor = jnp.exp(block_log[:, None] - running_log)
    key_to_end = key_float * end_factor
    lower_mask = jnp.tril(jnp.ones((BLOCK, BLOCK), jnp.float32))
    scores = (
        jnp.einsum("nihc,njhc->nhij", query_decayed, key_inverse, precision=precise) * lower_mask
    )
    inner_part = jnp.einsum("nhij,njhv->nihv", scores, value_float, precision=precise)
    increment = jnp.einsum("njhc,njhv->nhcv", key_to_end, value_float, precision=precise)
    block_decay = jnp.exp(block_log)
    zero_state = jnp.zeros((heads_local, DK, DV), jnp.float32)
    local_total, local_prev = lax.scan(advance, zero_state, (block_decay, increment))
    device_decay = jnp.exp(jnp.sum(block_log, axis=0))
    prior_factor = jnp.exp(jnp.cumsum(block_log, axis=0) - block_log)
    decay_pieces = jnp.broadcast_to(
        device_decay.reshape(experts, -1, 1), (experts, heads_local * DK // experts, 128)
    )
    (decay_mine,) = exchange([decay_pieces], False, 5)
    incoming = prefix(local_total, decay_mine, False, 0)
    state_prev = local_prev + prior_factor[:, :, :, None] * incoming[None]
    state_end = device_decay[:, :, None] * incoming + local_total
    raw_out = inner_part + jnp.einsum(
        "nihc,nhcv->nihv", query_decayed, state_prev, precision=precise
    )
    inverse_root = lax.rsqrt(jnp.mean(raw_out * raw_out, axis=-1, keepdims=True) + epsilon)
    normed = raw_out * inverse_root
    normed_rows = normed.astype(jnp.bfloat16).reshape(local_tokens, heads_local * DV)
    gate_local = gate_weight[0]
    up_local = up_weight[0]
    down_local = down_weight[0]
    row_send, scaled_send, normed_rows = lax.optimization_barrier(
        (row_send, scaled_send, normed_rows)
    )
    both_rows, both_scaled = exchange([row_send, scaled_send], True, 2)
    both_rows, both_scaled, normed_rows = lax.optimization_barrier(
        (both_rows, both_scaled, normed_rows)
    )
    normed_all = lax.all_gather(normed_rows, "sp", axis=0, tiled=True)
    totals, partial_value = expert_work(
        both_rows.reshape(-1, model_width),
        both_scaled.reshape(-1, model_width),
        gate_local,
        up_local,
        down_local,
    )
    halves = partial_value.astype(jnp.bfloat16).reshape(experts, 2, capacity, model_width)
    core = lax.axis_index("tp")
    kept = lax.dynamic_index_in_dim(halves, core, 1, keepdims=False)
    given = lax.dynamic_index_in_dim(halves, 1 - core, 1, keepdims=False)
    taken = lax.ppermute(given, "tp", [(0, 1), (1, 0)])
    summed = (kept.astype(jnp.float32) + taken.astype(jnp.float32)).astype(jnp.bfloat16)
    (expert_rows,) = exchange([summed], False, 3)
    picked = lax.dot_general(
        either,
        expert_rows.reshape(experts * capacity, model_width),
        contract_rows,
        preferred_element_type=jnp.float32,
    )
    token_back = (cotangent.astype(jnp.float32) + picked).astype(jnp.bfloat16)
    token_all = lax.all_gather(token_back, "tp", axis=0, tiled=True)
    back_normed = jnp.dot(token_all, out_weight, preferred_element_type=jnp.float32).reshape(
        block_count, BLOCK, heads_local, DV
    )
    back_raw = inverse_root * (
        back_normed - normed * jnp.mean(back_normed * normed, axis=-1, keepdims=True)
    )
    block_back = jnp.einsum("nihc,nihv->nhcv", query_decayed, back_raw, precision=precise)
    device_back = jnp.sum(prior_factor[:, :, :, None] * block_back, axis=0)
    future_state = prefix(device_back, decay_mine, True, 1)
    token_pieces = token_back.reshape(row_count, experts, -1).transpose(1, 0, 2)
    (token_slice,) = exchange([token_pieces], True, 4)
    out_total = lax.dot_general(
        token_slice.reshape(normed_all.shape[0], -1),
        normed_all,
        contract_rows,
        preferred_element_type=jnp.float32,
    )
    start_state, future_blocks = lax.scan(
        advance, future_state, (block_decay, block_back), reverse=True
    )
    value_dots = (
        jnp.einsum("nihv,njhv->nhij", back_raw, value_float, precision=precise) * lower_mask
    )
    query_part = jnp.einsum("nhij,njhc->nihc", value_dots, key_inverse, precision=precise)
    query_part = query_part + jnp.einsum("nihv,nhcv->nihc", back_raw, state_prev, precision=precise)
    query_back = query_part * jnp.exp(running_log)
    key_back = jnp.exp(-running_log) * jnp.einsum(
        "nhij,nihc->njhc", value_dots, query_decayed, precision=precise
    )
    key_back = key_back + end_factor * jnp.einsum(
        "nhcv,njhv->njhc", future_blocks, value_float, precision=precise
    )
    value_back = jnp.einsum("nhij,nihv->njhv", scores, back_raw, precision=precise)
    value_back = value_back + jnp.einsum(
        "njhc,nhcv->njhv", key_to_end, future_blocks, precision=precise
    )
    running_back = query_scaled * query_back - key_float * key_back
    within_block = jnp.einsum("ji,njhc->nihc", lower_mask, running_back, precision=precise)
    block_sums = jnp.sum(running_back, axis=1)
    strict_upper = jnp.triu(jnp.ones((block_count, block_count), jnp.float32), 1)
    later_blocks = jnp.einsum("nm,mhc->nhc", strict_upper, block_sums, precision=precise)
    cross_term = jnp.sum(state_end * future_state, axis=-1)
    decay_back = within_block + later_blocks[:, None] + cross_term[None, None]
    query_out = (
        (query_back * DK ** (-0.5)).astype(jnp.bfloat16).reshape(local_tokens, heads_local * DK)
    )
    key_out = key_back.astype(jnp.bfloat16).reshape(local_tokens, heads_local * DK)
    value_out = value_back.astype(jnp.bfloat16).reshape(local_tokens, heads_local * DV)
    decay_out = decay_back.reshape(local_tokens, heads_local * DK)
    return (totals[0], totals[1], totals[2], out_total, query_out, key_out, value_out, decay_out)


def solution(mesh):
    in_specs = (
        P(("sp", "tp"), None),
        P(("sp", "tp"), None),
        P(("sp", "tp"), None),
        P(("sp", "tp"), None),
        P("sp", None, "tp"),
        P("sp", None, "tp"),
        P("sp", "tp", None),
        P(None, "tp"),
        P("sp", "tp"),
        P("sp", "tp"),
        P("sp", "tp"),
        P("sp", "tp"),
    )
    out_specs = (
        P("sp", None, "tp"),
        P("sp", None, "tp"),
        P("sp", "tp", None),
        P("sp", "tp"),
        P("sp", "tp"),
        P("sp", "tp"),
        P("sp", "tp"),
        P("sp", "tp"),
    )
    return jax.shard_map(body, mesh=mesh, in_specs=in_specs, out_specs=out_specs, check_vma=False)
```

profile of v0, /device:TPU:0, one launch (start us, length us, event | category | flops | bytes accessed | tf_op | source)
XLA Modules:
  0.0 282.8 jit_solution(142013397068470403)
XLA Ops:
  20.4 4.2 %while.30 = (s32[]{:T(128)}, f32[4,128,256]{2,1,0:T(8,128)S(1)}, f32[2,4,128,256]{3,2,1,0:T(8,128)}, f32[2,4,128]{2,1,0:T(4,128)S(1)}, f32[2,4,128,256]{3,2,1,0:T(8,128)}, /*index=5*/s32[]{:T(128)}, s32[]{:T(128)}) while((s32[]{:T(128)}, f32[4,128,256]{2,1,0:T(8,128)S(1)}, f32[2,4,128,256]{3,2,1,0:T(8,128)}, ...), condition=%wide.region_4.5_spmd.clone, body=%wide.region_3.4_spmd.clone.sunk | while | flops 524291 | bytes 2627692 | solution.py:327
  26.3 13.4 %exchange_5.1.decay_ref = f32[16,32,128]{2,1,0:T(8,128)} custom-call(f32[16,32,128]{2,1,0:T(8,128)} %broadcast_in_dim.83.refs_0_), custom_call_target="tpu_custom_call" | custom-call | tf_op jit(solution)/shard_map/exchange_5/pallas_call | solution.py:139
  39.6 21.5 %prefix_0.1 = bf16[16,32,256]{2,1,0:T(8,128)(2,1)} custom-call(bf16[16,32,256]{2,1,0:T(8,128)(2,1)} %bitcast.185, f32[16,32,128]{2,1,0:T(8,128)} %exchange_5.1.decay_ref), custom_call_target="tpu_custom_call" | custom-call | tf_op jit(solution)/shard_map/prefix_0/pallas_call | solution.py:204
  62.2 2.3 multiply_reduce_fusion.3
  68.8 46.8 %exchange_2.1 = (bf16[16,2,16,2048]{3,2,1,0:T(8,128)(2,1)}, bf16[16,2,16,2048]{3,2,1,0:T(8,128)(2,1)}) custom-call(bf16[16,16,2048]{2,1,0:T(8,128)(2,1)} %bitcast.178, bf16[16,16,2048]{2,1,0:T(8,128)(2,1)} %bitcast.177), custom_call_target="tpu_custom_call" | custom-call | tf_op jit(solution)/shard_map/exchange_2/pallas_call | solution.py:139
  115.7 3.0 %fusion.8 = f32[512,512]{1,0:T(8,128)S(1)} fusion(bf16[512,2048]{1,0:T(8,128)(2,1)} %bitcast.197, bf16[1,2048,512]{2,1,0:T(8,128)(2,1)S(1)} %copy-done), kind=kOutput, calls=%fused_computation.21 | convolution fusion | flops 1073741824 | bytes 5242880 | tf_op jit(solution)/shard_map/dot_general | solution.py:231
  121.7 2.4 multiply_convert_fusion.1
  124.8 3.3 %fusion.6 = f32[512,2048]{1,0:T(8,128)} fusion(bf16[512,512]{1,0:T(8,128)(2,1)S(1)} %get-tuple-element.199, bf16[1,2048,512]{2,1,0:T(8,128)(2,1)S(1)} %copy-done), kind=kOutput, calls=%fused_computation.19 | convolution fusion | flops 1073741824 | bytes 6815744 | tf_op jit(solution)/shard_map/dot_general | solution.py:245
  128.1 5.7 %add_convert_fusion = bf16[512,2048]{1,0:T(8,128)(2,1)} fusion(f32[512,2048]{1,0:T(8,128)} %fusion.6, bf16[512,512]{1,0:T(8,128)(2,1)} %get-tuple-element.198, bf16[1,2048,512]{2,1,0:T(8,128)(2,1)} %param.21), kind=kOutput, calls=%fused_computation.6 | convolution fusion | flops 1075838976 | bytes 8912896 | tf_op jit(solution)/shard_map/dot_general | solution.py:248
  133.9 2.3 dynamic-slice_bitcast_fusion.2
  136.6 4.4 %fusion = bf16[1,2048,512]{2,1,0:T(8,128)(2,1)} fusion(bf16[512,2048]{1,0:T(8,128)(2,1)} %bitcast.198, bf16[512,512]{1,0:T(8,128)(2,1)} %copy-done.21), kind=kOutput, calls=%fused_computation.10 | convolution fusion | flops 1074790400 | bytes 4718592 | tf_op jit(solution)/shard_map/dot_general | solution.py:240
  141.1 2.6 fusion.1
  143.7 2.7 fusion.2
  146.4 2.6 fusion.5.refs_0_
  149.0 32.3 %exchange_3.1 = bf16[16,16,2048]{2,1,0:T(8,128)(2,1)} custom-call(bf16[16,16,2048]{2,1,0:T(8,128)(2,1)} %fusion.5.refs_0_), custom_call_target="tpu_custom_call" | custom-call | tf_op jit(solution)/shard_map/exchange_3/pallas_call | solution.py:139
  181.3 1.9 fusion.4
  184.8 30.2 %exchange_4.1 = bf16[16,2,64,128]{3,2,1,0:T(8,128)(2,1)} custom-call(bf16[16,64,128]{2,1,0:T(8,128)(2,1)} %bitcast_bitcast_fusion.refs_0_), custom_call_target="tpu_custom_call" | custom-call | tf_op jit(solution)/shard_map/exchange_4/pallas_call | solution.py:139
  215.0 2.4 all_gather.7
  217.4 3.7 %fusion.77 = f32[128,1024]{1,0:T(8,128)} fusion(bf16[128,2048]{1,0:T(8,128)(2,1)S(1)} %all_gather.7, bf16[2048,1024]{1,0:T(8,128)(2,1)} %param.23), kind=kOutput, calls=%fused_computation.130 | convolution fusion | flops 536870912 | bytes 5242880 | tf_op jit(solution)/shard_map/dot_general | solution.py:376
  221.1 2.1 reshape.162
  226.6 2.4 multiply_reduce_fusion
  229.0 23.9 %prefix_1.1 = bf16[16,32,256]{2,1,0:T(8,128)(2,1)} custom-call(bf16[16,32,256]{2,1,0:T(8,128)(2,1)} %bitcast.186, f32[16,32,128]{2,1,0:T(8,128)} %exchange_5.1.decay_ref), custom_call_target="tpu_custom_call" | custom-call | tf_op jit(solution)/shard_map/prefix_1/pallas_call | solution.py:204
  259.1 4.1 %while.29 = (s32[]{:T(128)}, f32[4,128,256]{2,1,0:T(8,128)S(1)}, f32[2,4,128,256]{3,2,1,0:T(8,128)}, f32[2,4,128]{2,1,0:T(4,128)S(1)}, f32[2,4,128,256]{3,2,1,0:T(8,128)}, /*index=5*/s32[]{:T(128)}) while((s32[]{:T(128)}, f32[4,128,256]{2,1,0:T(8,128)S(1)}, f32[2,4,128,256]{3,2,1,0:T(8,128)}, f32[2,4,128]{2,1,0:T(4,128)S(1)}, ...), condition=%wide.region_11.12_spmd, body=%wide.region_10.11_spmd.sunk | while | flops 262147 | bytes 2627685 | solution.py:393
  272.2 3.7 %fusion.76 = f32[128,1024]{1,0:T(8,128)} fusion(bf16[2048,128]{1,0:T(8,128)(2,1)S(1)} %bitcast.184, bf16[2048,1024]{1,0:T(8,128)(2,1)} %all-gather.2.cloned.1.call-done), kind=kOutput, calls=%fused_computation.129 | convolution fusion | flops 536870912 | bytes 5242880 | tf_op jit(solution)/shard_map/dot_general | solution.py:387
  (146 shorter events, 52.2 us)
Async XLA Ops:
  7.2 108.5 %copy-start = (bf16[1,2048,512]{2,1,0:T(8,128)(2,1)S(1)}, bf16[1,2048,512]{2,1,0:T(8,128)(2,1)}, u32[]{:S(2)}) copy-start(bf16[1,2048,512]{2,1,0:T(8,128)(2,1)} %param.20) | copy-start | bytes 6291460
  7.2 265.0 %all-gather.2.cloned.1.call-start = ((), (), s32[]{:S(2)}) async-start(), calls=%async_computation | async-start | bytes 4456448 | tf_op jit(solution)/shard_map/all_gather | solution.py:353
  12.4 6.9 %copy-start.5 = (f32[2,64,4,128]{3,2,1,0:T(4,128)}, f32[2,64,4,128]{3,2,1,0:T(4,128)S(1)}, u32[]{:S(2)}) copy-start(f32[2,64,4,128]{3,2,1,0:T(4,128)S(1)} %reshape.170) | copy-start | bytes 786436
  15.4 4.0 %copy-start.8 = (bf16[2,64,4,256]{3,2,1,0:T(4,128)(2,1)}, bf16[2,64,4,256]{3,2,1,0:T(4,128)(2,1)S(1)}, u32[]{:S(2)}) copy-start(bf16[2,64,4,256]{3,2,1,0:T(4,128)(2,1)S(1)} %reshape.153) | copy-start | bytes 786436
  16.8 3.6 %copy-start.15 = (f32[2,4,64,64]{3,2,1,0:T(8,128)}, f32[2,4,64,64]{3,2,1,0:T(8,128)S(1)}, u32[]{:S(2)}) copy-start(f32[2,4,64,64]{3,2,1,0:T(8,128)S(1)} %convolution_multiply_fusion.2) | copy-start | bytes 393220
  62.1 2.7 copy-start.11
  62.2 3.5 %copy-start.24 = (bf16[64,2048]{1,0:T(8,128)(2,1)S(1)}, bf16[64,2048]{1,0:T(8,128)(2,1)}, u32[]{:S(2)}) copy-start(bf16[64,2048]{1,0:T(8,128)(2,1)} %param.16) | copy-start | bytes 786436
  64.5 2.8 copy-start.22
  115.6 3.0 %copy-start.19 = (bf16[1,2048,512]{2,1,0:T(8,128)(2,1)S(1)}, bf16[1,2048,512]{2,1,0:T(8,128)(2,1)}, u32[]{:S(2)}) copy-start(bf16[1,2048,512]{2,1,0:T(8,128)(2,1)} %param.21) | copy-start | bytes 6291460
  115.7 3.0 %copy-start.28 = (bf16[16,2,16,2048]{3,2,1,0:T(8,128)(2,1)S(1)}, bf16[16,2,16,2048]{3,2,1,0:T(8,128)(2,1)}, u32[]{:S(2)}) copy-start(bf16[16,2,16,2048]{3,2,1,0:T(8,128)(2,1)} %get-tuple-element.154) | copy-start | bytes 6291460
  118.7 3.0 %copy-start.26 = (bf16[16,2,16,2048]{3,2,1,0:T(8,128)(2,1)S(1)}, bf16[16,2,16,2048]{3,2,1,0:T(8,128)(2,1)}, u32[]{:S(2)}) copy-start(bf16[16,2,16,2048]{3,2,1,0:T(8,128)(2,1)} %get-tuple-element.155) | copy-start | bytes 6291460
  120.0 4.1 %copy-start.32 = (f32[512,512]{1,0:T(8,128)}, f32[512,512]{1,0:T(8,128)S(1)}, u32[]{:S(2)}) copy-start(f32[512,512]{1,0:T(8,128)S(1)} %fusion.11) | copy-start | bytes 3145732
  136.2 10.2 %collective-permute-start = (bf16[16,16,2048]{2,1,0:T(8,128)(2,1)}, bf16[16,16,2048]{2,1,0:T(8,128)(2,1)}, u32[]{:S(2)}, u32[]{:S(2)}) collective-permute-start(bf16[16,16,2048]{2,1,0:T(8,128)(2,1)} %dynamic-slice_bitcast_fusion.2), channel_id=1, source_target_pairs={{0,1},{1,0},{2,3},{3,2},{4,5},{5,4},{6,7},{7,6},{8,9},{9,8},{10,11... | collective-permute-start | bytes 3145736 | tf_op jit(solution)/shard_map/ppermute | solution.py:365
  136.6 4.4 %copy-start.23 = (bf16[512,512]{1,0:T(8,128)(2,1)S(1)}, bf16[512,512]{1,0:T(8,128)(2,1)}, u32[]{:S(2)}) copy-start(bf16[512,512]{1,0:T(8,128)(2,1)} %get-tuple-element.198) | copy-start | bytes 1572868
  136.6 4.4 %copy-start.29 = (bf16[16,2,16,2048]{3,2,1,0:T(8,128)(2,1)S(1)}, bf16[16,2,16,2048]{3,2,1,0:T(8,128)(2,1)}, u32[]{:S(2)}) copy-start(bf16[16,2,16,2048]{3,2,1,0:T(8,128)(2,1)} %get-tuple-element.154) | copy-start | bytes 6291460
  141.0 2.7 copy-start.27
  141.0 2.7 copy-start.31
  143.7 2.7 copy-start.7
  223.2 3.4 %copy-start.9 = (f32[2,64,4,128]{3,2,1,0:T(4,128)S(1)}, f32[2,64,4,128]{3,2,1,0:T(4,128)}, u32[]{:S(2)}) copy-start(f32[2,64,4,128]{3,2,1,0:T(4,128)} %mul.191) | copy-start | bytes 786436
  263.3 3.9 %copy-start.6 = (f32[2,64,4,128]{3,2,1,0:T(4,128)S(1)}, f32[2,64,4,128]{3,2,1,0:T(4,128)}, u32[]{:S(2)}) copy-start(f32[2,64,4,128]{3,2,1,0:T(4,128)} %copy-done.5) | copy-start | bytes 786436
  263.3 3.9 %copy-start.10 = (f32[2,64,4,128]{3,2,1,0:T(4,128)S(1)}, f32[2,64,4,128]{3,2,1,0:T(4,128)}, u32[]{:S(2)}) copy-start(f32[2,64,4,128]{3,2,1,0:T(4,128)} %mul.191) | copy-start | bytes 786436
  263.3 3.9 %copy-start.18 = (f32[2,4,64,64]{3,2,1,0:T(8,128)S(1)}, f32[2,4,64,64]{3,2,1,0:T(8,128)}, u32[]{:S(2)}) copy-start(f32[2,4,64,64]{3,2,1,0:T(8,128)} %copy-done.17) | copy-start | bytes 393220
  265.3 2.7 copy-start.16
  268.9 3.3 %copy-start.20 = (bf16[16,2,64,128]{3,2,1,0:T(8,128)(2,1)S(1)}, bf16[16,2,64,128]{3,2,1,0:T(8,128)(2,1)}, u32[]{:S(2)}) copy-start(bf16[16,2,64,128]{3,2,1,0:T(8,128)(2,1)} %exchange_4.1) | copy-start | bytes 1572868
  (12 other events, 18.2 us)
Sparse Core Ops, SparseCore 0:
  115.8 99.8 all-gather.1
where the time goes:
time: 284 us; the launch traced here: 283 us
  Pallas kernels  168 us (59%)
  matrix products  55.4 us (20%)
  local copies, waits for them, and re-layouts  24.7 us (9%)
  other arithmetic  17 us (6%)
  between operations  14.7 us (5%)
    pallas_call x4, Pallas kernels, exchange(): pl.pallas_call(functools.partial(exchange_kernel, total, pair), out_shape...  123 us
    pallas_call x2, Pallas kernels, prefix(): pl.pallas_call(functools.partial(prefix_kernel, backward), out_shape=jax....  45.5 us
    unnamed x72, local copies, waits for them, and re-layouts  7.85 us
    dot_general x1, matrix products, expert_work(): lax.dot_general(back_up, up_local, contract_cols, preferred_element_type=...  5.73 us
  transfers between devices with their start and end apart: 2, of which 0 were waited for; matrix products, arithmetic and copies ran while one was open for 22% of the time, Pallas kernels for 31%

commit v1 on v0

v1 whole, which is shorter than its diff:
```python
import functools

import jax
import jax.numpy as jnp
from jax import lax
from jax.experimental import pallas as pl
from jax.experimental.pallas import tpu as pltpu
from jax.sharding import PartitionSpec as P

DK = 128
DV = 256
BLOCK = 64
GROUPS = 4

MESH = pl.DeviceIdType.MESH
F32 = jnp.float32
BF16 = jnp.bfloat16
epsilon = 1e-06
NN = (((1,), (0,)), ((), ()))
NT = (((1,), (1,)), ((), ()))
TN = (((0,), (0,)), ((), ()))
VMEM = pltpu.VMEM


def mm(a, b, dims=NN):
    return lax.dot_general(a, b, dims, preferred_element_type=F32)


def split2(x):
    high = x.astype(BF16)
    return (high, (x - high.astype(F32)).astype(BF16))


def split3(x):
    high, _ = split2(x)
    rest = x - high.astype(F32)
    return (high,) + split2(rest)


def mm3(a, b, dims=NN):
    return mm(a[0], b[0], dims) + (mm(a[0], b[1], dims) + mm(a[1], b[0], dims))


def mm2l(a, b, dims=NN):
    return mm(a[0], b, dims) + mm(a[1], b, dims)


def mm2r(a, b, dims=NN):
    return mm(a, b[0], dims) + mm(a, b[1], dims)


def place():
    count = lax.axis_size("sp")
    plane = count // GROUPS
    mine = lax.axis_index("sp")
    return (count, plane, mine, mine // plane, lax.rem(mine, plane), lax.axis_index("tp"))


def loop(low, high, act):
    def turn(step, carry):
        act(step)
        return carry

    lax.fori_loop(low, high, turn, 0)


def signal(where):
    pl.semaphore_signal(
        pltpu.get_barrier_semaphore(), inc=1, device_id=where, device_id_type=MESH
    )


def greet_all():
    count, plane, mine, z, p, core = place()
    loop(1, count, lambda step: signal({"sp": lax.rem(mine + step, count)}))
    signal({"tp": 1 - core})


def greet_near():
    count, plane, mine, z, p, core = place()
    loop(1, plane, lambda step: signal({"sp": z * plane + lax.rem(p + step, plane)}))
    loop(1, GROUPS, lambda step: signal({"sp": lax.rem(z + step, GROUPS) * plane + p}))
    signal({"tp": 1 - core})


def met(total):
    pl.semaphore_wait(pltpu.get_barrier_semaphore(), total)


def send(source, target, send_sem, recv_sem, where):
    return pltpu.make_async_remote_copy(
        src_ref=source,
        dst_ref=target,
        send_sem=send_sem,
        recv_sem=recv_sem,
        device_id=where,
        device_id_type=MESH,
    )


def tri(size, lower, strict=False):
    row = lax.broadcasted_iota(jnp.int32, (size, size), 0)
    col = lax.broadcasted_iota(jnp.int32, (size, size), 1)
    if lower:
        return row > col if strict else row >= col
    return row <= col


def head_parts(rl, q, k, h, mid_row):
    cols = slice(h * DK, (h + 1) * DK)
    rl_h = rl[:, cols]
    mid = rl_h[mid_row : mid_row + 1]
    last = rl_h[rl_h.shape[0] - 1 :]
    qs = q[:, cols].astype(F32) * DK ** (-0.5)
    kf = k[:, cols].astype(F32)
    return (rl_h, mid, last, qs, kf)


def scatter_pieces(target, value, h):
    count, rows = target.shape[0], target.shape[1]
    cols = slice(h * DK, (h + 1) * DK)
    for j in range(count):
        target[j, :, cols] = value[j * rows : (j + 1) * rows].astype(target.dtype)


class Scan:
    def __init__(self, total, got, ready, out, decs, s1, r1, s2, r2, backward):
        self.refs = (total, got, ready, out, decs)
        self.sems = (s1, r1, s2, r2)
        self.backward = backward

    def first(self, step, there):
        total, got, ready, out, decs = self.refs
        count, plane, mine, z, p, core = place()
        ahead = lax.rem(mine + step, count)
        return send(
            total.at[ahead], got.at[there], self.sems[0].at[step], self.sems[1].at[step], {"sp": ahead}
        )

    def second(self, step, there):
        total, got, ready, out, decs = self.refs
        count, plane, mine, z, p, core = place()
        ahead = lax.rem(mine + step, count)
        return send(
            ready.at[ahead], out.at[there], self.sems[2].at[step], self.sems[3].at[step], {"sp": ahead}
        )

    def start(self):
        total, got, ready, out, decs = self.refs
        count, plane, mine, z, p, core = place()
        loop(1, count, lambda step: self.first(step, mine).start())
        got[mine] = total[mine]

    def middle(self):
        total, got, ready, out, decs = self.refs
        count, plane, mine, z, p, core = place()
        loop(1, count, lambda step: self.first(step, lax.rem(mine + count - step, count)).wait_recv())

        def turn(position, carry):
            index = count - 1 - position if self.backward else position
            ready[index] = carry.astype(ready.dtype)
            return carry * decs[index] + got[index].astype(F32)

        lax.fori_loop(0, count, turn, jnp.zeros(got.shape[1:], F32))
        loop(1, count, lambda step: self.second(step, mine).start())
        out[mine] = ready[mine]

    def finish(self):
        count, plane, mine, z, p, core = place()
        loop(1, count, lambda step: self.second(step, lax.rem(mine + count - step, count)).wait_recv())

    def settle(self):
        count, plane, mine, z, p, core = place()

        def act(step):
            self.first(step, mine).wait_send()
            self.second(step, mine).wait_send()

        loop(1, count, act)


def front_kernel(
    mid_ref, cot_ref, ex_ref, wt_ref, q_ref, k_ref, v_ref, ld_ref,
    rows_ref, meta_ref, pick_ref, decs_ref, inc_ref, normed_ref, normed_rows_ref, inv_ref, rl_ref, score_ref, total_ref,
    pack, pack_meta, zbuf, wide, piece, got, ready, dec_mine,
    zs_sem, zr_sem, xs_sem, xr_sem, fs_sem, fr_sem, l_sem, s1, r1, s2, r2, ds, dr,
):
    count, plane, mine, z, p, core = place()
    tokens = mid_ref.shape[0]
    cap = rows_ref.shape[4]
    gcap = plane * cap // 2
    greet_all()

    lane = lax.broadcasted_iota(jnp.int32, (tokens, 128), 1)
    e0, e1 = ex_ref[:, 0:1], ex_ref[:, 1:2]
    w0, w1 = wt_ref[:, 0:1], wt_ref[:, 1:2]
    hit0, hit1 = (e0 == lane), (e1 == lane)
    earlier = tri(tokens, True, True).astype(F32).astype(BF16)
    named = (hit0.astype(F32) + hit1.astype(F32)).astype(BF16)
    before = mm(earlier, named)
    rank0 = jnp.sum(jnp.where(hit0, before, 0.0), axis=1, keepdims=True)
    rank1 = jnp.sum(jnp.where(hit1, before, 0.0), axis=1, keepdims=True)
    member = ((e0 >= lane * plane) & (e0 < lane * plane + plane)).astype(F32)
    ahead_count = mm(earlier, member.astype(BF16))
    rank_group = jnp.sum(member * ahead_count, axis=1, keepdims=True)
    group = jnp.sum(member * lane.astype(F32), axis=1, keepdims=True)
    lane_f = lane.astype(F32)
    pick = (group * gcap + rank_group == lane_f).astype(F32).astype(BF16)
    pick_ref[...] = pick
    slot0 = (e0.astype(F32) - group * plane) * cap + rank0
    slot1 = (e1.astype(F32) - group * plane) * cap + rank1
    weights = jnp.where(slot0 == lane_f, w0, 0.0) + jnp.where(slot1 == lane_f, w1, 0.0)
    parts = split3(weights)
    packed_meta = mm(pick, parts[0], TN) + (mm(pick, parts[1], TN) + mm(pick, parts[2], TN))
    pack_meta[...] = packed_meta.reshape(pack_meta.shape)
    for kind, ref in enumerate((mid_ref, cot_ref)):
        chosen = mm(pick, ref[...], TN).astype(BF16)
        for g in range(GROUPS):
            pack[g, kind] = chosen[g * gcap : (g + 1) * gcap]
    met(count)

    def z_copy(step, there):
        target = lax.rem(z + step, GROUPS)
        return send(
            pack.at[target], zbuf.at[there], zs_sem.at[0, step], zr_sem.at[0, step], {"sp": target * plane + p}
        )

    def z_meta(step, there):
        target = lax.rem(z + step, GROUPS)
        return send(
            pack_meta.at[target], meta_ref.at[there], zs_sem.at[1, step], zr_sem.at[1, step],
            {"sp": target * plane + p},
        )

    for step in (2, 1, 3):
        z_meta(step, z).start()
        z_copy(step, z).start()
    meta_ref[z] = pack_meta[z]

    def x_copy(kind, turn, source, step, there):
        target = lax.rem(p + step, plane)
        return send(
            wide.at[turn, kind, target], rows_ref.at[kind, core, source, there],
            xs_sem.at[kind, turn, step], xr_sem.at[kind, turn, step], {"sp": z * plane + target},
        )

    def own_copy(kind, turn, source):
        return pltpu.make_async_copy(
            wide.at[turn, kind, p], rows_ref.at[kind, core, source, p], l_sem.at[kind, turn]
        )

    def expand(turn, source, mid, cot):
        table = meta_ref[source][:, : plane * cap]
        chosen = (table > 0).astype(F32).astype(BF16)
        ones = jnp.ones((gcap, 128), BF16)
        t3 = split3(table)
        column = (mm(t3[0], ones, TN) + (mm(t3[1], ones, TN) + mm(t3[2], ones, TN)))[:, :1]
        width = mid.shape[1]
        chunk = 512
        for n in range(0, width, chunk):
            cols = slice(n, n + chunk)
            wide[turn, 0, :, :, cols] = (
                mm(chosen, mid[:, cols], TN).reshape(plane, cap, chunk).astype(BF16)
            )
            wide[turn, 1, :, :, cols] = (
                (column * mm(chosen, cot[:, cols], TN)).reshape(plane, cap, chunk).astype(BF16)
            )
        for kind in range(2):
            loop(1, plane, lambda step: x_copy(kind, turn, source, step, p).start())
            own_copy(kind, turn, source).start()

    expand(0, z, pack.at[z, 0], pack.at[z, 1])

    length = q_ref.shape[0]
    heads = q_ref.shape[1] // DK
    mid_row = length // 2 - 1
    low = tri(length, True)
    low_b = low.astype(F32).astype(BF16)
    l3 = split3(ld_ref[...])
    rl = mm(low_b, l3[0]) + (mm(low_b, l3[1]) + mm(low_b, l3[2]))
    rl_ref[...] = rl
    dec_mine[...] = jnp.exp(rl[length - 1 :])
    def d_copy(step, there):
        target = lax.rem(mine + step, count)
        return send(dec_mine, decs_ref.at[there], ds.at[step], dr.at[step], {"sp": target})

    loop(1, count, lambda step: d_copy(step, mine).start())
    decs_ref[mine] = dec_mine[...]
    for h in range(heads):
        rl_h, mid, last, qs, kf = head_parts(rl, q_ref, k_ref, h, mid_row)
        value = v_ref[:, h * DV : (h + 1) * DV]
        to_end = split2(kf * jnp.exp(last - rl_h))
        total = mm2r(value, to_end, TN)
        total_ref[:, h * DK : (h + 1) * DK] = total
        scatter_pieces(piece, total, h)
    scan = Scan(piece, got, ready, inc_ref, decs_ref, s1, r1, s2, r2, False)
    scan.start()
    for h in range(heads):
        rl_h, mid, last, qs, kf = head_parts(rl, q_ref, k_ref, h, mid_row)
        up = split2(qs * jnp.exp(rl_h - mid))
        down = split2(kf * jnp.exp(mid - rl_h))
        score_ref[h] = jnp.where(low, mm3(up, down, NT), 0.0)

    for turn in range(1, GROUPS):
        step = (2, 1, 3)[turn - 1]
        source = lax.rem(z + GROUPS - step, GROUPS)
        z_meta(step, source).wait_recv()
        z_copy(step, source).wait_recv()
        expand(turn, source, zbuf.at[source, 0], zbuf.at[source, 1])

    loop(1, count, lambda step: d_copy(step, lax.rem(mine + count - step, count)).wait_recv())
    scan.middle()

    def forward(kind, turn, source, side):
        return send(
            rows_ref.at[kind, side, source], rows_ref.at[kind, side, source],
            fs_sem.at[kind, turn], fr_sem.at[kind, turn], {"tp": 1 - core},
        )

    for turn in range(GROUPS):
        source = lax.rem(z + GROUPS - (0, 2, 1, 3)[turn], GROUPS)
        for kind in range(2):
            own_copy(kind, turn, source).wait()
            loop(
                1, plane,
                lambda step: x_copy(kind, turn, source, step, lax.rem(p + plane - step, plane)).wait_recv(),
            )
            forward(kind, turn, source, core).start()

    scan.finish()
    for h in range(heads):
        rl_h, mid, last, qs, kf = head_parts(rl, q_ref, k_ref, h, mid_row)
        value = v_ref[:, h * DV : (h + 1) * DV]
        decayed = split2(qs * jnp.exp(rl_h))
        state = inc_ref[:, :, h * DK : (h + 1) * DK].reshape(DV, DK)
        raw = mm2l(split2(score_ref[h]), value) + mm2l(decayed, state, NT)
        inverse = lax.rsqrt(jnp.mean(raw * raw, axis=1, keepdims=True) + epsilon)
        out = raw * inverse
        normed_ref[:, h * DV : (h + 1) * DV] = out
        normed_rows_ref[:, h * DV : (h + 1) * DV] = out.astype(BF16)
        inv_ref[:, h * 128 : (h + 1) * 128] = jnp.broadcast_to(inverse, (length, 128))

    for turn in range(GROUPS):
        source = lax.rem(z + GROUPS - (0, 2, 1, 3)[turn], GROUPS)
        for kind in range(2):
            forward(kind, turn, source, core).wait_send()
            forward(kind, turn, source, 1 - core).wait_recv()
            loop(1, plane, lambda step: x_copy(kind, turn, source, step, p).wait_send())
    for step in (2, 1, 3):
        z_meta(step, z).wait_send()
        z_copy(step, z).wait_send()
    loop(1, count, lambda step: d_copy(step, mine).wait_send())
    scan.settle()


def front(mid, cot, experts, weights, q, k, v, ld):
    count = lax.axis_size("sp")
    plane = count // GROUPS
    rows, width = mid.shape
    cap = 4 * rows // count
    gcap = plane * cap // 2
    length, keys = q.shape
    heads = keys // DK
    dma = pltpu.SemaphoreType.DMA
    shape = jax.ShapeDtypeStruct
    vrows = DV // count
    outs = [
        shape((2, 2, GROUPS, plane, cap, width), BF16),
        shape((GROUPS, gcap, 128), F32),
        shape((rows, GROUPS * gcap), BF16),
        shape((count, 1, keys), F32),
        shape((count, vrows, keys), BF16),
        shape((length, heads * DV), F32),
        shape((length, heads * DV), BF16),
        shape((length, heads * 128), F32),
        shape((length, keys), F32),
        shape((heads, length, length), F32),
        shape((DV, keys), F32),
    ]
    return pl.pallas_call(
        front_kernel,
        out_shape=outs,
        in_specs=[pl.BlockSpec(memory_space=VMEM)] * 8,
        out_specs=[pl.BlockSpec(memory_space=VMEM)] * len(outs),
        scratch_shapes=[
            VMEM((GROUPS, 2, gcap, width), BF16),
            VMEM((GROUPS, gcap, 128), F32),
            VMEM((GROUPS, 2, gcap, width), BF16),
            VMEM((GROUPS, 2, plane, cap, width), BF16),
            VMEM((count, vrows, keys), BF16),
            VMEM((count, vrows, keys), BF16),
            VMEM((count, vrows, keys), BF16),
            VMEM((1, keys), F32),
            dma((2, GROUPS)), dma((2, GROUPS)),
            dma((2, GROUPS, plane)), dma((2, GROUPS, plane)),
            dma((2, GROUPS)), dma((2, GROUPS)), dma((2, GROUPS)),
            dma((count,)), dma((count,)), dma((count,)), dma((count,)), dma((count,)), dma((count,)),
        ],
        compiler_params=pltpu.CompilerParams(collective_id=0, has_side_effects=True),
        name="front",
    )(mid, cot, experts, weights, q, k, v, ld)


def expert_kernel(
    rows_ref, gate_ref, up_ref, down_ref, meta_ref, pick_ref, cot_ref, normed_ref,
    gate_out, up_out, down_out, token_ref, near_ref,
    hidden, back_gate, back_up, part, taken, whole, landed, comb, home,
    ns, nr, ps, pr, es, er, cs, cr,
):
    count, plane, mine, z, p, core = place()
    gcap = comb.shape[1]
    cap = whole.shape[2]
    half = part.shape[1] * part.shape[2]
    group_rows = part.shape[2]
    width = rows_ref.shape[2]
    hide = gate_ref.shape[1]
    greet_near()
    met(plane + GROUPS - 1)

    def n_copy(step, there):
        target = lax.rem(p + step, plane)
        return send(normed_ref, near_ref.at[there], ns.at[step], nr.at[step], {"sp": z * plane + target})

    loop(1, plane, lambda step: n_copy(step, p).start())
    near_ref[p] = normed_ref[...]

    def p_copy(g):
        return send(part.at[1 - core, g], taken.at[g], ps.at[g], pr.at[g], {"tp": 1 - core})

    def compute(side):
        base = pl.multiple_of(side * half, half)
        span = pl.ds(base, half)

        def inner(n):
            cols = pl.ds(pl.multiple_of(n * 256, 256), 256)
            pre_gate = mm(rows_ref[0, span, :], gate_ref[:, cols])
            pre_up = mm(rows_ref[0, span, :], up_ref[:, cols])
            back = mm(rows_ref[1, span, :], down_ref[cols, :], NT)
            sig = jax.nn.sigmoid(pre_gate)
            swish = pre_gate * sig
            hidden[span, cols] = (swish * pre_up).astype(BF16)
            back_up[span, cols] = (back * swish).astype(BF16)
            back_gate[span, cols] = (back * pre_up * (sig * (1.0 + pre_gate * (1.0 - sig)))).astype(BF16)

        loop(0, hide // 256, inner)

        def outer(n):
            cols = pl.ds(pl.multiple_of(n * 256, 256), 256)
            value = mm(back_gate[span, :], gate_ref[cols, :], NT) + mm(back_up[span, :], up_ref[cols, :], NT)
            part[side, :, :, cols] = value.astype(BF16).reshape(GROUPS, group_rows, 256)

        loop(0, width // 256, outer)

    compute(1 - core)
    order = [lax.rem(z + step, GROUPS) for step in (2, 1, 3, 0)]
    for g in order:
        p_copy(g).start()
    compute(core)

    def e_copy(turn, g, step, there):
        target = lax.rem(p + step, plane)
        return send(
            whole.at[turn, target], landed.at[turn, there], es.at[turn, step], er.at[turn, step],
            {"sp": z * plane + target},
        )

    for turn, g in enumerate(order):
        p_copy(g).wait_recv()
        value = part[core, g].astype(F32) + taken[g].astype(F32)
        whole[turn] = value.astype(BF16).reshape(plane, cap, width)
        loop(1, plane, lambda step: e_copy(turn, g, step, p).start())
        landed[turn, p] = whole[turn, p]

    def gates(n):
        cols = pl.ds(pl.multiple_of(n * 256, 256), 256)
        gate_out[cols, :] = mm(rows_ref[0, :, cols], back_gate[...], TN).astype(BF16)
        up_out[cols, :] = mm(rows_ref[0, :, cols], back_up[...], TN).astype(BF16)

    loop(0, width // 256, gates)

    def c_copy(turn, g, there):
        return send(comb.at[turn], home.at[there], cs.at[turn], cr.at[turn], {"sp": g * plane + p})

    for turn, g in enumerate(order):
        loop(1, plane, lambda step: e_copy(turn, g, step, lax.rem(p + plane - step, plane)).wait_recv())
        table = meta_ref[g][:, : plane * cap]
        chosen = (table > 0).astype(F32).astype(BF16)
        value = mm(chosen, landed[turn].reshape(plane * cap, width)).astype(BF16)
        if turn < GROUPS - 1:
            comb[turn] = value
            c_copy(turn, g, z).start()
        else:
            home[z] = value

    def downs(n):
        cols = pl.ds(pl.multiple_of(n * 256, 256), 256)
        down_out[cols, :] = mm(hidden[:, cols], rows_ref[1], TN).astype(BF16)

    loop(0, hide // 256, downs)

    for turn in range(GROUPS - 1):
        step = (2, 1, 3)[turn]
        c_copy(turn, z, lax.rem(z + GROUPS - step, GROUPS)).wait_recv()
    token_ref[...] = (
        cot_ref[...].astype(F32) + mm(pick_ref[...], home[...].reshape(GROUPS * gcap, width))
    ).astype(BF16)

    for turn, g in enumerate(order):
        p_copy(g).wait_send()
        loop(1, plane, lambda step: e_copy(turn, g, step, p).wait_send())
        if turn < GROUPS - 1:
            c_copy(turn, g, z).wait_send()
    loop(1, plane, lambda step: n_copy(step, p).wait_send())
    loop(1, plane, lambda step: n_copy(step, lax.rem(p + plane - step, plane)).wait_recv())


def experts_stage(rows, gate, up, down, meta, pick, cot, normed_rows):
    count = lax.axis_size("sp")
    plane = count // GROUPS
    cap = rows.shape[4]
    width = rows.shape[5]
    rows = rows.reshape(2, -1, width)
    total = rows.shape[1]
    hide = gate.shape[1]
    gcap = meta.shape[1]
    dma = pltpu.SemaphoreType.DMA
    shape = jax.ShapeDtypeStruct
    outs = [
        shape(gate.shape, BF16),
        shape(up.shape, BF16),
        shape(down.shape, BF16),
        shape(cot.shape, BF16),
        shape((plane,) + normed_rows.shape, BF16),
    ]
    return pl.pallas_call(
        expert_kernel,
        out_shape=outs,
        in_specs=[pl.BlockSpec(memory_space=VMEM)] * 8,
        out_specs=[pl.BlockSpec(memory_space=VMEM)] * len(outs),
        scratch_shapes=[
            VMEM((total, hide), BF16),
            VMEM((total, hide), BF16),
            VMEM((total, hide), BF16),
            VMEM((2, GROUPS, plane * cap, width), BF16),
            VMEM((GROUPS, plane * cap, width), BF16),
            VMEM((GROUPS, plane, cap, width), BF16),
            VMEM((GROUPS, plane, cap, width), BF16),
            VMEM((GROUPS - 1, gcap, width), BF16),
            VMEM((GROUPS, gcap, width), BF16),
            dma((plane,)), dma((plane,)),
            dma((GROUPS,)), dma((GROUPS,)),
            dma((GROUPS, plane)), dma((GROUPS, plane)),
            dma((GROUPS,)), dma((GROUPS,)),
        ],
        compiler_params=pltpu.CompilerParams(collective_id=1, has_side_effects=True),
        name="experts",
    )(rows, gate, up, down, meta, pick, cot, normed_rows)


def back_kernel(
    token_ref, weight_ref, near_ref, normed_ref, inv_ref, rl_ref, score_ref, inc_ref, decs_ref, total_ref,
    q_ref, k_ref, v_ref,
    out_ref, dq_ref, dk_ref, dv_ref, da_ref,
    both, cut, tok, own, give, take, raw, piece, got, ready, fut, run,
    ts, tr, ks, kr, os, orr, s1, r1, s2, r2,
):
    count, plane, mine, z, p, core = place()
    rows, width = token_ref.shape
    share = width // count
    length = q_ref.shape[0]
    heads = q_ref.shape[1] // DK
    mid_row = length // 2 - 1
    greet_all()
    met(count)

    def t_copy(side):
        return send(token_ref, both.at[side], ts, tr, {"tp": 1 - core})

    t_copy(core).start()
    both[core] = token_ref[...]
    t_copy(1 - core).wait_recv()

    for other in range(plane):
        for g in range(GROUPS):
            start = (g * plane + other) * share
            for side in range(2):
                cut[other, side * rows : (side + 1) * rows, g * share : (g + 1) * share] = both[
                    side, :, start : start + share
                ]

    def k_copy(step, there):
        target = lax.rem(p + step, plane)
        return send(cut.at[target], tok.at[there], ks.at[step], kr.at[step], {"sp": z * plane + target})

    loop(1, plane, lambda step: k_copy(step, p).start())
    tok[p] = cut[p]

    rl = rl_ref[...]
    for h in range(heads):
        cols = slice(h * DV, (h + 1) * DV)
        back = mm(both[...].reshape(length, width), weight_ref[:, cols])
        normed = normed_ref[:, cols]
        mean = jnp.mean(back * normed, axis=1, keepdims=True)
        inverse = inv_ref[:, h * 128 : h * 128 + 1]
        value = inverse * (back - normed * mean)
        raw[:, cols] = value
        rl_h, mid, last, qs, kf = head_parts(rl, q_ref, k_ref, h, mid_row)
        scatter_pieces(piece, mm3(split2(value), split2(qs * jnp.exp(rl_h)), TN), h)
    scan = Scan(piece, got, ready, fut, decs_ref, s1, r1, s2, r2, True)
    scan.start()

    def o_copy(step, there):
        target = lax.rem(z + step, GROUPS)
        return send(give.at[target], take.at[there], os.at[step], orr.at[step], {"sp": target * plane + p})

    loop(1, plane, lambda step: k_copy(step, lax.rem(p + plane - step, plane)).wait_recv())
    near = near_ref[...].reshape(plane * length, near_ref.shape[2])
    for g in range(GROUPS):
        value = mm(tok[:, :, g * share : (g + 1) * share].reshape(plane * length, share), near, TN)
        own[g] = value
        give[g] = value.astype(BF16)

    low = tri(length, True)
    scan.middle()
    for step in (2, 1, 3):
        o_copy(step, z).start()

    def parts(h):
        rl_h, mid, last, qs, kf = head_parts(rl, q_ref, k_ref, h, mid_row)
        cols = slice(h * DK, (h + 1) * DK)
        wide = slice(h * DV, (h + 1) * DV)
        return (rl_h, mid, last, qs, kf, cols, wide, v_ref[:, wide], split2(raw[:, wide]))

    for h in range(heads):
        rl_h, mid, last, qs, kf, cols, wide, value, back = parts(h)
        dots = split2(jnp.where(low, mm2l(back, value, NT), 0.0))
        up_scale, down_scale = jnp.exp(rl_h - mid), jnp.exp(mid - rl_h)
        state = inc_ref[:, :, cols].reshape(DV, DK)
        dq = up_scale * mm3(dots, split2(kf * down_scale)) + jnp.exp(rl_h) * mm2l(back, state)
        dq_ref[:, cols] = (dq * DK ** (-0.5)).astype(BF16)
        dk = down_scale * mm3(dots, split2(qs * up_scale), TN)
        run[0, :, cols] = dk
        run[1, :, cols] = qs * dq
        own_value = mm3(split2(score_ref[h]), back, TN)
        raw[:, wide] = own_value

    scan.finish()
    high_b = tri(length, False).astype(F32).astype(BF16)
    for h in range(heads):
        rl_h, mid, last, qs, kf = head_parts(rl, q_ref, k_ref, h, mid_row)
        cols = slice(h * DK, (h + 1) * DK)
        wide = slice(h * DV, (h + 1) * DV)
        value = v_ref[:, wide]
        future = fut[:, :, cols].reshape(DV, DK)
        to_end = jnp.exp(last - rl_h)
        dk = run[0, :, cols] + to_end * mm(value, future)
        dk_ref[:, cols] = dk.astype(BF16)
        dv_ref[:, wide] = (raw[:, wide] + mm2l(split2(kf * to_end), future, NT)).astype(BF16)
        change = run[1, :, cols] - kf * dk
        c3 = split3(change)
        later = mm(high_b, c3[0]) + (mm(high_b, c3[1]) + mm(high_b, c3[2]))
        state = inc_ref[:, :, cols].reshape(DV, DK).astype(F32)
        end = jnp.exp(last) * state + total_ref[:, cols]
        cross = jnp.sum(end * future.astype(F32), axis=0, keepdims=True)
        da_ref[:, cols] = later + cross

    for step in (2, 1, 3):
        o_copy(step, lax.rem(z + GROUPS - step, GROUPS)).wait_recv()
    sides = [lax.rem(z + step, GROUPS) for step in (1, 2, 3)]
    out_ref[...] = (own[z] + take[sides[0]].astype(F32)) + (
        take[sides[1]].astype(F32) + take[sides[2]].astype(F32)
    )

    t_copy(core).wait_send()
    loop(1, plane, lambda step: k_copy(step, p).wait_send())
    for step in (2, 1, 3):
        o_copy(step, z).wait_send()
    scan.settle()


def back_stage(token, weight, near, normed, inv, rl, score, inc, decs, total, q, k, v):
    count = lax.axis_size("sp")
    plane = count // GROUPS
    rows, width = token.shape
    share = width // count
    length, keys = q.shape
    values = v.shape[1]
    vrows = DV // count
    dma = pltpu.SemaphoreType.DMA
    shape = jax.ShapeDtypeStruct
    outs = [
        shape((share, values), F32),
        shape(q.shape, BF16),
        shape(k.shape, BF16),
        shape(v.shape, BF16),
        shape(q.shape, F32),
    ]
    return pl.pallas_call(
        back_kernel,
        out_shape=outs,
        in_specs=[pl.BlockSpec(memory_space=VMEM)] * 13,
        out_specs=[pl.BlockSpec(memory_space=VMEM)] * len(outs),
        scratch_shapes=[
            VMEM((2, rows, width), BF16),
            VMEM((plane, length, GROUPS * share), BF16),
            VMEM((plane, length, GROUPS * share), BF16),
            VMEM((GROUPS, share, values), F32),
            VMEM((GROUPS, share, values), BF16),
            VMEM((GROUPS, share, values), BF16),
            VMEM((length, values), F32),
            VMEM((count, vrows, keys), BF16),
            VMEM((count, vrows, keys), BF16),
            VMEM((count, vrows, keys), BF16),
            VMEM((count, vrows, keys), BF16),
            VMEM((2, length, keys), F32),
            dma, dma,
            dma((plane,)), dma((plane,)),
            dma((GROUPS,)), dma((GROUPS,)),
            dma((count,)), dma((count,)), dma((count,)), dma((count,)),
        ],
        compiler_params=pltpu.CompilerParams(collective_id=2, has_side_effects=True),
        name="back",
    )(token, weight, near, normed, inv, rl, score, inc, decs, total, q, k, v)


def body(
    mid_rows,
    cotangent,
    route_experts,
    route_weights,
    gate_weight,
    up_weight,
    down_weight,
    out_weight,
    queries,
    key_rows,
    value_rows,
    log_decay,
):
    rows, meta, pick, decs, inc, normed, normed_rows, inv, rl, score, total = front(
        mid_rows, cotangent, route_experts, route_weights, queries, key_rows, value_rows, log_decay
    )
    gate_grad, up_grad, down_grad, token, near = experts_stage(
        rows, gate_weight[0], up_weight[0], down_weight[0], meta, pick, cotangent, normed_rows
    )
    out_grad, dq, dk, dv, da = back_stage(
        token, out_weight, near, normed, inv, rl, score, inc, decs, total, queries, key_rows, value_rows
    )
    return (gate_grad[None], up_grad[None], down_grad[None], out_grad, dq, dk, dv, da)


def solution(mesh):
    in_specs = (
        P(("sp", "tp"), None),
        P(("sp", "tp"), None),
        P(("sp", "tp"), None),
        P(("sp", "tp"), None),
        P("sp", None, "tp"),
        P("sp", None, "tp"),
        P("sp", "tp", None),
        P(None, "tp"),
        P("sp", "tp"),
        P("sp", "tp"),
        P("sp", "tp"),
        P("sp", "tp"),
    )
    out_specs = (
        P("sp", None, "tp"),
        P("sp", None, "tp"),
        P("sp", "tp", None),
        P("sp", "tp"),
        P("sp", "tp"),
        P("sp", "tp"),
        P("sp", "tp"),
        P("sp", "tp"),
    )
    return jax.shard_map(body, mesh=mesh, in_specs=in_specs, out_specs=out_specs, check_vma=False)
```

time: 284 us -> 158 us (0.56)
  matrix products: 55.4 us -> 0 us
  Pallas kernels: 168 us -> 143 us
  other arithmetic: 17 us -> 0 us
  between operations: 14.7 us -> 0.69 us
  local copies, waits for them, and re-layouts: 24.7 us -> 12.3 us
    dot_general x27 -> x0, matrix products: 55.4 us -> none  [the longest x1 5.73 us: expert_work(): lax.dot_general(back_up, up_local, contract_cols, preferred_element_type=...]
    pallas_call x6 -> x3, Pallas kernels: 168 us -> 143 us  [the longest x1 56 us: front(): pl.pallas_call(front_kernel, out_shape=outs, in_specs=[pl.BlockSpec(memor...]
    reshape x5 -> x0, local copies, waits for them, and re-layouts: 6.1 us -> none  [the longest x1 2.07 us: body(): jnp.dot(token_all, out_weight, preferred_element_type=jnp.float32)]
    add x5 -> x0, other arithmetic: 5.5 us -> none  [the longest x4 4.8 us: advance(): return (factor[:, :, None] * carry_state + addend, carry_state)]
    unnamed x72 -> x26, local copies, waits for them, and re-layouts: 7.85 us -> 12.3 us
    convert_element_type x3 -> x0, other arithmetic: 3.49 us -> none  [the longest x1 2.62 us: body(): (kept.astype(jnp.float32) + taken.astype(jnp.float32)).astype(jnp.bfloat16)]
    mul x3 -> x0, other arithmetic: 3.26 us -> none  [the longest x1 1.25 us: body(): inverse_root * (back_normed - normed * jnp.mean(back_normed * normed, axi...]
  transfers between devices with their start and end apart: 2 -> 0, of which waited for: 0 -> 0; matrix products, arithmetic and copies ran while one was open for 22% -> 0% of each run, Pallas kernels for 31% -> 0%
where the time goes in v1:
time: 158 us; the launch traced here: 156 us
  Pallas kernels  143 us (91%)
  local copies, waits for them, and re-layouts  12.3 us (8%)
    pallas_call x1, Pallas kernels, front(): pl.pallas_call(front_kernel, out_shape=outs, in_specs=[pl.BlockSpec(memor...  56 us
    pallas_call x1, Pallas kernels, back_stage(): pl.pallas_call(back_kernel, out_shape=outs, in_specs=[pl.BlockSpec(memory...  46 us
    pallas_call x1, Pallas kernels, experts_stage(): pl.pallas_call(expert_kernel, out_shape=outs, in_specs=[pl.BlockSpec(memo...  40.5 us
    unnamed x26, local copies, waits for them, and re-layouts  12.3 us

profile of v1, /device:TPU:0, one launch (start us, length us, event | category | flops | bytes accessed | tf_op | source)
XLA Modules:
  0.0 155.5 jit_solution(17314485917553532688)
XLA Ops:
  0.6 1.4 copy.20.ex_ref
  2.0 1.4 copy.21.wt_ref
  3.4 56.0 %front.1 = (bf16[2,2,4,4,16,2048]{5,4,3,2,1,0:T(8,128)(2,1)}, f32[4,32,128]{2,1,0:T(8,128)}, bf16[64,128]{1,0:T(8,128)(2,1)}, f32[16,1,512]{2,1,0:T(1,128)}, bf1...) custom-call(bf16[64,2048]{1,0:T(8,128)(2,1)} %mid_ref.1, ...), custom_call_target="tpu_custom_call" | custom-call | tf_op jit(solution)/shard_map/front/pallas_call | solution.py:380
  59.4 40.5 %experts.1 = (bf16[2048,512]{1,0:T(8,128)(2,1)}, bf16[2048,512]{1,0:T(8,128)(2,1)}, bf16[512,2048]{1,0:T(8,128)(2,1)}, bf16[64,2048]{1,0:T(8,128)(2,1)}, bf16[4,128,1024]{2,1,0:T(8,128)(2,1)}) custom-call(bf16[2,512,2048]{2,1,0:T(8,128)(2,1)} %bitcast.7, bf16[2048,512]{1,0:T(8,128)(2,1)} %bitcast.11, bf16[2048,512]{1,0:T(8,128)(2,1)} %bitcast.12, ...), custom_call_target="tpu_custom_call" | custom-call | tf_op jit(solution)/shard_map/experts/pallas_call | solution.py:535
  99.9 0.0 copy-start.2
  99.9 46.0 %back.1 = (f32[128,1024]{1,0:T(8,128)}, bf16[128,512]{1,0:T(8,128)(2,1)}, bf16[128,512]{1,0:T(8,128)(2,1)}, bf16[128,1024]{1,0:T(8,128)(2,1)}, f32[128,512]{1,0:T(8,128)}) custom-call(bf16[64,2048]{1,0:T(8,128)(2,1)} %get-tuple-element.36.token_ref, bf16[2048,1024]{1,0:T(8,128)(2,1)} %weight_ref.1, bf16[4,128,1024]{2,1,0:T(8,128)(2,1)} %get-tuple-element.37.near_ref, ...), custom_call_target="tpu_custom_call" | custom-call | tf_op jit(solution)/shard_map/back/pallas_call | solution.py:698
  145.9 0.0 copy-done.2
  145.9 0.0 copy-start.1
  146.0 1.3 copy.30
  147.3 1.0 copy-done.1
  148.3 0.0 copy-start
  148.3 1.3 copy.31
  149.6 1.0 copy-done
  150.7 1.3 copy.32
  152.0 0.0 copy-done.3
  152.0 0.8 copy.33
  152.8 0.0 copy-done.7
  152.8 0.7 copy.34
  153.4 0.0 copy-done.6
  153.4 0.7 copy.35
  154.1 0.0 copy-done.5
  154.1 0.7 copy.36
  154.8 0.0 copy-done.4
  154.8 0.7 copy.37
  (5 shorter events, 0.0 us)
Async XLA Ops:
  99.9 46.0 %copy-start.2 = (bf16[2048,512]{1,0:T(8,128)(2,1)S(1)}, bf16[2048,512]{1,0:T(8,128)(2,1)}, u32[]{:S(2)}) copy-start(bf16[2048,512]{1,0:T(8,128)(2,1)} %get-tuple-element.33) | copy-start | bytes 6291460
  145.9 2.3 %copy-start.1 = (bf16[2048,512]{1,0:T(8,128)(2,1)S(1)}, bf16[2048,512]{1,0:T(8,128)(2,1)}, u32[]{:S(2)}) copy-start(bf16[2048,512]{1,0:T(8,128)(2,1)} %get-tuple-element.34) | copy-start | bytes 6291460
  148.3 2.3 %copy-start = (bf16[512,2048]{1,0:T(8,128)(2,1)S(1)}, bf16[512,2048]{1,0:T(8,128)(2,1)}, u32[]{:S(2)}) copy-start(bf16[512,2048]{1,0:T(8,128)(2,1)} %get-tuple-element.35) | copy-start | bytes 6291460
  150.6 1.3 copy-start.3
  150.6 2.1 %copy-start.7 = (bf16[128,512]{1,0:T(8,128)(2,1)S(1)}, bf16[128,512]{1,0:T(8,128)(2,1)}, u32[]{:S(2)}) copy-start(bf16[128,512]{1,0:T(8,128)(2,1)} %get-tuple-element.62) | copy-start | bytes 393220
  150.6 2.8 %copy-start.6 = (bf16[128,512]{1,0:T(8,128)(2,1)S(1)}, bf16[128,512]{1,0:T(8,128)(2,1)}, u32[]{:S(2)}) copy-start(bf16[128,512]{1,0:T(8,128)(2,1)} %get-tuple-element.63) | copy-start | bytes 393220
  150.6 3.5 %copy-start.5 = (bf16[128,1024]{1,0:T(8,128)(2,1)S(1)}, bf16[128,1024]{1,0:T(8,128)(2,1)}, u32[]{:S(2)}) copy-start(bf16[128,1024]{1,0:T(8,128)(2,1)} %get-tuple-element.64) | copy-start | bytes 786436
  152.0 2.8 %copy-start.4 = (f32[128,512]{1,0:T(8,128)S(1)}, f32[128,512]{1,0:T(8,128)}, u32[]{:S(2)}) copy-start(f32[128,512]{1,0:T(8,128)} %get-tuple-element.65) | copy-start | bytes 786436

commit v2 on v1

v2 whole, which is shorter than its diff:
```python
import functools
import types

import jax
import jax.numpy as jnp
from jax import lax
from jax.experimental import pallas as pl
from jax.experimental.pallas import tpu as pltpu
from jax.sharding import PartitionSpec as P

DK = 128
DV = 256
BLOCK = 64
GROUPS = 4

MESH = pl.DeviceIdType.MESH
F32 = jnp.float32
BF16 = jnp.bfloat16
epsilon = 1e-06
NN = (((1,), (0,)), ((), ()))
NT = (((1,), (1,)), ((), ()))
TN = (((0,), (0,)), ((), ()))
VMEM = pltpu.VMEM


def mm(a, b, dims=NN):
    return lax.dot_general(a, b, dims, preferred_element_type=F32)


def split2(x):
    high = x.astype(BF16)
    return (high, (x - high.astype(F32)).astype(BF16))


def split3(x):
    high, _ = split2(x)
    rest = x - high.astype(F32)
    return (high,) + split2(rest)


def mm3(a, b, dims=NN):
    return mm(a[0], b[0], dims) + (mm(a[0], b[1], dims) + mm(a[1], b[0], dims))


def mm2l(a, b, dims=NN):
    return mm(a[0], b, dims) + mm(a[1], b, dims)


def mm2r(a, b, dims=NN):
    return mm(a, b[0], dims) + mm(a, b[1], dims)


def place():
    count = lax.axis_size("sp")
    plane = count // GROUPS
    mine = lax.axis_index("sp")
    return (count, plane, mine, mine // plane, lax.rem(mine, plane), lax.axis_index("tp"))


def loop(low, high, act):
    def turn(step, carry):
        act(step)
        return carry

    lax.fori_loop(low, high, turn, 0)


def signal(where):
    pl.semaphore_signal(
        pltpu.get_barrier_semaphore(), inc=1, device_id=where, device_id_type=MESH
    )


def greet_all():
    count, plane, mine, z, p, core = place()
    loop(1, count, lambda step: signal({"sp": lax.rem(mine + step, count)}))
    signal({"tp": 1 - core})


def greet_near():
    count, plane, mine, z, p, core = place()
    loop(1, plane, lambda step: signal({"sp": z * plane + lax.rem(p + step, plane)}))
    loop(1, GROUPS, lambda step: signal({"sp": lax.rem(z + step, GROUPS) * plane + p}))
    signal({"tp": 1 - core})


def met(total):
    pl.semaphore_wait(pltpu.get_barrier_semaphore(), total)


def send(source, target, send_sem, recv_sem, where):
    return pltpu.make_async_remote_copy(
        src_ref=source,
        dst_ref=target,
        send_sem=send_sem,
        recv_sem=recv_sem,
        device_id=where,
        device_id_type=MESH,
    )


def tri(size, lower, strict=False):
    row = lax.broadcasted_iota(jnp.int32, (size, size), 0)
    col = lax.broadcasted_iota(jnp.int32, (size, size), 1)
    if lower:
        return row > col if strict else row >= col
    return row <= col


def head_parts(rl, q, k, h, mid_row):
    cols = slice(h * DK, (h + 1) * DK)
    rl_h = rl[:, cols]
    mid = rl_h[mid_row : mid_row + 1]
    last = rl_h[rl_h.shape[0] - 1 :]
    qs = q[:, cols].astype(F32) * DK ** (-0.5)
    kf = k[:, cols].astype(F32)
    return (rl_h, mid, last, qs, kf)


def scatter_pieces(target, value, h):
    count, rows = target.shape[0], target.shape[1]
    cols = slice(h * DK, (h + 1) * DK)
    for j in range(count):
        target[j, :, cols] = value[j * rows : (j + 1) * rows].astype(target.dtype)


class Scan:
    def __init__(self, total, got, ready, out, decs, s1, r1, s2, r2, backward):
        self.refs = (total, got, ready, out, decs)
        self.sems = (s1, r1, s2, r2)
        self.backward = backward

    def first(self, step, there):
        total, got, ready, out, decs = self.refs
        count, plane, mine, z, p, core = place()
        ahead = lax.rem(mine + step, count)
        return send(
            total.at[ahead], got.at[there], self.sems[0].at[step], self.sems[1].at[step], {"sp": ahead}
        )

    def second(self, step, there):
        total, got, ready, out, decs = self.refs
        count, plane, mine, z, p, core = place()
        ahead = lax.rem(mine + step, count)
        return send(
            ready.at[ahead], out.at[there], self.sems[2].at[step], self.sems[3].at[step], {"sp": ahead}
        )

    def start(self):
        total, got, ready, out, decs = self.refs
        count, plane, mine, z, p, core = place()
        loop(1, count, lambda step: self.first(step, mine).start())
        got[mine] = total[mine]

    def middle(self):
        total, got, ready, out, decs = self.refs
        count, plane, mine, z, p, core = place()
        loop(1, count, lambda step: self.first(step, lax.rem(mine + count - step, count)).wait_recv())

        def turn(position, carry):
            index = count - 1 - position if self.backward else position
            ready[index] = carry.astype(ready.dtype)
            return carry * decs[index] + got[index].astype(F32)

        lax.fori_loop(0, count, turn, jnp.zeros(got.shape[1:], F32))
        loop(1, count, lambda step: self.second(step, mine).start())
        out[mine] = ready[mine]

    def finish(self):
        count, plane, mine, z, p, core = place()
        loop(1, count, lambda step: self.second(step, lax.rem(mine + count - step, count)).wait_recv())

    def settle(self):
        count, plane, mine, z, p, core = place()

        def act(step):
            self.first(step, mine).wait_send()
            self.second(step, mine).wait_send()

        loop(1, count, act)


STEPS = (0, 2, 1, 3)
FIRST = ("ex", "wt", "mid", "cot", "ld", "q", "k", "v")
LATER = ("gate", "up", "down", "weight")


def column(row, eye):
    return jnp.sum(jnp.where(eye, row, 0.0), axis=1, keepdims=True)


def whole_kernel(names, *refs):
    r = types.SimpleNamespace(**dict(zip(names, refs)))
    count, plane, mine, z, p, core = place()
    greet_all()
    tokens, width = r.mid.shape
    cap = r.rows.shape[4]
    gcap = plane * cap // 2
    slots = plane * cap
    hide = r.gate.shape[1]
    length = r.q.shape[0]
    heads = r.q.shape[1] // DK
    mid_row = length // 2 - 1
    share = width // count
    low = tri(length, True)
    source_of = [lax.rem(z + GROUPS - step, GROUPS) for step in STEPS]

    loads = {
        name: pltpu.make_async_copy(getattr(r, name + "_in"), getattr(r, name), r.load_sem.at[n])
        for n, name in enumerate(FIRST + LATER)
    }
    for name in FIRST:
        loads[name].start()
    for name in FIRST[:4]:
        loads[name].wait()

    lane = lax.broadcasted_iota(jnp.int32, (tokens, 128), 1)
    lane_f = lane.astype(F32)
    eye = lax.broadcasted_iota(jnp.int32, (tokens, tokens), 0) == lax.broadcasted_iota(
        jnp.int32, (tokens, tokens), 1
    )
    chosen_experts = r.ex[...].astype(F32)
    e0, e1 = column(chosen_experts[0:1], eye), column(chosen_experts[1:2], eye)
    w0, w1 = column(r.wt[0:1, :], eye), column(r.wt[1:2, :], eye)
    hit0, hit1 = (e0 == lane_f), (e1 == lane_f)
    earlier = tri(tokens, True, True).astype(F32).astype(BF16)
    first_lane = lane_f * plane
    member = ((e0 >= first_lane) & (e0 < first_lane + plane)).astype(F32)
    named = (hit0.astype(F32) + hit1.astype(F32)).astype(BF16)
    before = mm(earlier, named)
    ahead_count = mm(earlier, member.astype(BF16))
    rank_group = jnp.sum(member * ahead_count, axis=1, keepdims=True)
    group = jnp.sum(member * lane_f, axis=1, keepdims=True)
    pick = (group * gcap + rank_group == lane_f).astype(F32).astype(BF16)
    r.pick[...] = pick
    for kind, ref in enumerate((r.mid, r.cot)):
        chosen = mm(pick, ref[...], TN).astype(BF16)
        for g in range(GROUPS):
            r.pack[g, kind] = chosen[g * gcap : (g + 1) * gcap]
    rank0 = jnp.sum(jnp.where(hit0, before, 0.0), axis=1, keepdims=True)
    rank1 = jnp.sum(jnp.where(hit1, before, 0.0), axis=1, keepdims=True)
    slot0 = (e0 - group * plane) * cap + rank0
    slot1 = (e1 - group * plane) * cap + rank1
    weights = jnp.where(slot0 == lane_f, w0, 0.0) + jnp.where(slot1 == lane_f, w1, 0.0)
    w3 = split3(weights)
    packed_meta = mm(pick, w3[0], TN) + (mm(pick, w3[1], TN) + mm(pick, w3[2], TN))
    r.pack_meta[...] = packed_meta.reshape(r.pack_meta.shape)
    met(count)

    def z_copy(step, there):
        target = lax.rem(z + step, GROUPS)
        return send(
            r.pack.at[target], r.zbuf.at[there], r.zs.at[0, step], r.zr.at[0, step],
            {"sp": target * plane + p},
        )

    def z_meta(step, there):
        target = lax.rem(z + step, GROUPS)
        return send(
            r.pack_meta.at[target], r.meta.at[there], r.zs.at[1, step], r.zr.at[1, step],
            {"sp": target * plane + p},
        )

    for step in STEPS[1:]:
        z_meta(step, z).start()
        z_copy(step, z).start()
    r.meta[z] = r.pack_meta[z]
    for name in LATER:
        loads[name].start()

    def x_copy(kind, turn, step, there):
        target = lax.rem(p + step, plane)
        return send(
            r.wide.at[turn, kind, target], r.rows.at[kind, turn, core, there],
            r.xs.at[kind, turn, step], r.xr.at[kind, turn, step], {"sp": z * plane + target},
        )

    def own_copy(kind, turn):
        return pltpu.make_async_copy(
            r.wide.at[turn, kind, p], r.rows.at[kind, turn, core, p], r.own_sem.at[kind, turn]
        )

    def expand(turn, mid, cot):
        table = r.meta[source_of[turn]][:, :slots]
        chosen = (table > 0).astype(F32).astype(BF16)
        ones = jnp.ones((gcap, 128), BF16)
        t3 = split3(table)
        scale = (mm(t3[0], ones, TN) + (mm(t3[1], ones, TN) + mm(t3[2], ones, TN)))[:, :1]
        chunk = 512
        for kind, ref in enumerate((mid, cot)):
            for n in range(0, width, chunk):
                cols = slice(n, n + chunk)
                value = mm(chosen, ref[:, cols], TN)
                if kind:
                    value = scale * value
                r.wide[turn, kind, :, :, cols] = value.reshape(plane, cap, chunk).astype(BF16)
            loop(1, plane, lambda step: x_copy(kind, turn, step, p).start())
            own_copy(kind, turn).start()

    def receive(turn):
        step, source = STEPS[turn], source_of[turn]
        z_meta(step, source).wait_recv()
        z_copy(step, source).wait_recv()
        expand(turn, r.zbuf.at[source, 0], r.zbuf.at[source, 1])

    def forward(kind, turn, side):
        return send(
            r.rows.at[kind, turn, side], r.rows.at[kind, turn, side],
            r.fs.at[kind, turn], r.fr.at[kind, turn], {"tp": 1 - core},
        )

    def arrive(turn):
        for kind in range(2):
            own_copy(kind, turn).wait()
            loop(
                1, plane,
                lambda step: x_copy(kind, turn, step, lax.rem(p + plane - step, plane)).wait_recv(),
            )
            forward(kind, turn, core).start()

    def p_copy(turn):
        return send(r.part.at[turn, 1 - core], r.taken.at[turn], r.ps.at[turn], r.pr.at[turn], {"tp": 1 - core})

    def compute(turn):
        for kind in range(2):
            forward(kind, turn, 1 - core).wait_recv()
        many = 2 * slots

        def inner(n):
            cols = pl.ds(pl.multiple_of(n * 256, 256), 256)
            rows = r.rows[0, turn].reshape(many, width)
            pre_gate = mm(rows, r.gate[:, cols])
            pre_up = mm(rows, r.up[:, cols])
            back = mm(r.rows[1, turn].reshape(many, width), r.down[cols, :], NT)
            sig = jax.nn.sigmoid(pre_gate)
            swish = pre_gate * sig
            r.hidden[turn, :, cols] = (swish * pre_up).astype(BF16)
            r.back_up[turn, :, cols] = (back * swish).astype(BF16)
            r.back_gate[turn, :, cols] = (back * pre_up * (sig * (1.0 + pre_gate * (1.0 - sig)))).astype(BF16)

        loop(0, hide // 256, inner)

        def outer(n):
            cols = pl.ds(pl.multiple_of(n * 512, 512), 512)
            value = mm(r.back_gate[turn], r.gate[cols, :], NT) + mm(r.back_up[turn], r.up[cols, :], NT)
            r.part[turn, :, :, cols] = value.astype(BF16).reshape(2, slots, 512)

        loop(0, width // 512, outer)
        p_copy(turn).start()

    def e_copy(turn, step, there):
        target = lax.rem(p + step, plane)
        return send(
            r.result.at[turn, target], r.landed.at[turn, there], r.es.at[turn, step], r.er.at[turn, step],
            {"sp": z * plane + target},
        )

    def give_back(turn):
        p_copy(turn).wait_recv()
        value = r.part[turn, core].astype(F32) + r.taken[turn].astype(F32)
        r.result[turn] = value.astype(BF16).reshape(plane, cap, width)
        loop(1, plane, lambda step: e_copy(turn, step, p).start())
        r.landed[turn, p] = r.result[turn, p]

    def c_copy(turn, there):
        return send(
            r.comb.at[turn], r.home.at[there], r.cs.at[turn], r.cr.at[turn],
            {"sp": source_of[turn] * plane + p},
        )

    def combine(turn):
        loop(1, plane, lambda step: e_copy(turn, step, lax.rem(p + plane - step, plane)).wait_recv())
        table = r.meta[source_of[turn]][:, :slots]
        chosen = (table > 0).astype(F32).astype(BF16)
        value = mm(chosen, r.landed[turn].reshape(slots, width)).astype(BF16)
        if turn:
            r.comb[turn] = value
            c_copy(turn, z).start()
        else:
            r.home[z] = value

    expand(0, r.pack.at[z, 0], r.pack.at[z, 1])

    for name in FIRST[4:]:
        loads[name].wait()
    low_b = low.astype(F32).astype(BF16)
    l3 = split3(r.ld[...])
    r.rl[...] = mm(low_b, l3[0]) + (mm(low_b, l3[1]) + mm(low_b, l3[2]))
    r.dec_mine[...] = jnp.exp(r.rl[length - 1 :, :])

    def d_copy(step, there):
        target = lax.rem(mine + step, count)
        return send(r.dec_mine, r.decs.at[there], r.ds.at[step], r.dr.at[step], {"sp": target})

    loop(1, count, lambda step: d_copy(step, mine).start())
    r.decs[mine] = r.dec_mine[...]

    def head(h):
        return head_parts(r.rl[...], r.q, r.k, h, mid_row)

    for h in range(heads):
        rl_h, mid, last, qs, kf = head(h)
        value = r.v[:, h * DV : (h + 1) * DV]
        to_end = split2(kf * jnp.exp(last - rl_h))
        total = mm2r(value, to_end, TN)
        r.total[:, h * DK : (h + 1) * DK] = total
        scatter_pieces(r.piece, total, h)
    scan = Scan(r.piece, r.got, r.ready, r.inc, r.decs, r.s1, r.r1, r.s2, r.r2, False)
    scan.start()

    arrive(0)
    receive(1)
    for name in LATER[:3]:
        loads[name].wait()
    compute(0)
    receive(2)
    arrive(1)
    give_back(0)
    compute(1)
    receive(3)
    arrive(2)
    give_back(1)
    combine(0)
    compute(2)
    loop(1, count, lambda step: d_copy(step, lax.rem(mine + count - step, count)).wait_recv())
    scan.middle()
    arrive(3)
    give_back(2)
    combine(1)
    compute(3)
    combine(2)
    give_back(3)

    scan.finish()

    def n_copy(step, there):
        target = lax.rem(p + step, plane)
        return send(r.normed_rows, r.near.at[there], r.ns.at[step], r.nr.at[step], {"sp": z * plane + target})

    for h in range(heads):
        rl_h, mid, last, qs, kf = head(h)
        wide = slice(h * DV, (h + 1) * DV)
        up = split2(qs * jnp.exp(rl_h - mid))
        down = split2(kf * jnp.exp(mid - rl_h))
        score = jnp.where(low, mm3(up, down, NT), 0.0)
        r.score[h] = score
        decayed = split2(qs * jnp.exp(rl_h))
        state = r.inc[:, :, h * DK : (h + 1) * DK].reshape(DV, DK)
        raw = mm2l(split2(score), r.v[:, wide]) + mm2l(decayed, state, NT)
        inverse = lax.rsqrt(jnp.mean(raw * raw, axis=1, keepdims=True) + epsilon)
        out = raw * inverse
        r.normed[:, wide] = out
        r.normed_rows[:, wide] = out.astype(BF16)
        r.inv[:, h * 128 : (h + 1) * 128] = jnp.broadcast_to(inverse, (length, 128))
    r.near[p] = r.normed_rows[...]
    loop(1, plane, lambda step: n_copy(step, p).start())

    combine(3)
    all_rows = GROUPS * 2 * slots

    def gates(n):
        cols = pl.ds(pl.multiple_of(n * 256, 256), 256)
        rows = r.rows[0, :, :, :, :, cols].reshape(all_rows, 256)
        r.gate_out[cols, :] = mm(rows, r.back_gate[...].reshape(all_rows, hide), TN).astype(BF16)
        r.up_out[cols, :] = mm(rows, r.back_up[...].reshape(all_rows, hide), TN).astype(BF16)

    loop(0, width // 256, gates)

    for turn in range(1, GROUPS):
        c_copy(turn, lax.rem(z + STEPS[turn], GROUPS)).wait_recv()
    token = (
        r.cot[...].astype(F32) + mm(r.pick[...], r.home[...].reshape(GROUPS * gcap, width))
    ).astype(BF16)
    r.token[...] = token
    r.both[core] = token

    def t_copy(side):
        return send(r.token, r.both.at[side], r.ts, r.tr, {"tp": 1 - core})

    t_copy(core).start()
    t_copy(1 - core).wait_recv()

    for other in range(plane):
        for g in range(GROUPS):
            start = (g * plane + other) * share
            for side in range(2):
                r.cut[other, side * tokens : (side + 1) * tokens, g * share : (g + 1) * share] = r.both[
                    side, :, start : start + share
                ]

    def k_copy(step, there):
        target = lax.rem(p + step, plane)
        return send(r.cut.at[target], r.tok.at[there], r.ks.at[step], r.kr.at[step], {"sp": z * plane + target})

    loop(1, plane, lambda step: k_copy(step, p).start())
    r.tok[p] = r.cut[p]

    loads["weight"].wait()
    for h in range(heads):
        wide = slice(h * DV, (h + 1) * DV)
        back = mm(r.both[...].reshape(length, width), r.weight[:, wide])
        normed = r.normed[:, wide]
        mean = jnp.mean(back * normed, axis=1, keepdims=True)
        inverse = r.inv[:, h * 128 : h * 128 + 1]
        value = inverse * (back - normed * mean)
        r.raw[:, wide] = value
        rl_h, mid, last, qs, kf = head(h)
        scatter_pieces(r.piece2, mm3(split2(value), split2(qs * jnp.exp(rl_h)), TN), h)
    scan2 = Scan(r.piece2, r.got2, r.ready2, r.fut, r.decs, r.s3, r.r3, r.s4, r.r4, True)
    scan2.start()

    def o_copy(step, there):
        target = lax.rem(z + step, GROUPS)
        return send(
            r.give.at[target], r.take.at[there], r.os.at[step], r.orr.at[step], {"sp": target * plane + p}
        )

    for h in range(heads):
        rl_h, mid, last, qs, kf = head(h)
        cols = slice(h * DK, (h + 1) * DK)
        wide = slice(h * DV, (h + 1) * DV)
        back = split2(r.raw[:, wide])
        dots = split2(jnp.where(low, mm2l(back, r.v[:, wide], NT), 0.0))
        up_scale, down_scale = jnp.exp(rl_h - mid), jnp.exp(mid - rl_h)
        state = r.inc[:, :, cols].reshape(DV, DK)
        dq = up_scale * mm3(dots, split2(kf * down_scale)) + jnp.exp(rl_h) * mm2l(back, state)
        r.dq[:, cols] = (dq * DK ** (-0.5)).astype(BF16)
        r.run[0, :, cols] = down_scale * mm3(dots, split2(qs * up_scale), TN)
        r.run[1, :, cols] = qs * dq
        r.raw[:, wide] = mm3(split2(r.score[h]), back, TN)

    loop(1, plane, lambda step: k_copy(step, lax.rem(p + plane - step, plane)).wait_recv())
    loop(1, plane, lambda step: n_copy(step, lax.rem(p + plane - step, plane)).wait_recv())
    near = r.near[...].reshape(plane * length, r.near.shape[2])
    for g in range(GROUPS):
        value = mm(r.tok[:, :, g * share : (g + 1) * share].reshape(plane * length, share), near, TN)
        r.own[g] = value
        r.give[g] = value.astype(BF16)
    o_copy(1, z).start()
    scan2.middle()
    o_copy(2, z).start()
    o_copy(3, z).start()

    def downs(n):
        cols = pl.ds(pl.multiple_of(n * 256, 256), 256)
        hidden = r.hidden[:, :, cols].reshape(all_rows, 256)
        r.down_out[cols, :] = mm(hidden, r.rows[1].reshape(all_rows, width), TN).astype(BF16)

    loop(0, hide // 256, downs)

    scan2.finish()
    high_b = tri(length, False).astype(F32).astype(BF16)
    for h in range(heads):
        rl_h, mid, last, qs, kf = head(h)
        cols = slice(h * DK, (h + 1) * DK)
        wide = slice(h * DV, (h + 1) * DV)
        future = r.fut[:, :, cols].reshape(DV, DK)
        to_end = jnp.exp(last - rl_h)
        dk = r.run[0, :, cols] + to_end * mm(r.v[:, wide], future)
        r.dk[:, cols] = dk.astype(BF16)
        r.dv[:, wide] = (r.raw[:, wide] + mm2l(split2(kf * to_end), future, NT)).astype(BF16)
        change = split3(r.run[1, :, cols] - kf * dk)
        later = mm(high_b, change[0]) + (mm(high_b, change[1]) + mm(high_b, change[2]))
        state = r.inc[:, :, cols].reshape(DV, DK).astype(F32)
        end = jnp.exp(last) * state + r.total[:, cols]
        r.da[:, cols] = later + jnp.sum(end * future.astype(F32), axis=0, keepdims=True)

    for step in STEPS[1:]:
        o_copy(step, lax.rem(z + GROUPS - step, GROUPS)).wait_recv()
    sides = [lax.rem(z + step, GROUPS) for step in (1, 2, 3)]
    r.out[...] = (r.own[z] + r.take[sides[0]].astype(F32)) + (
        r.take[sides[1]].astype(F32) + r.take[sides[2]].astype(F32)
    )

    for step in STEPS[1:]:
        z_meta(step, z).wait_send()
        z_copy(step, z).wait_send()
        o_copy(step, z).wait_send()
    for turn in range(GROUPS):
        for kind in range(2):
            loop(1, plane, lambda step: x_copy(kind, turn, step, p).wait_send())
            forward(kind, turn, core).wait_send()
        p_copy(turn).wait_send()
        loop(1, plane, lambda step: e_copy(turn, step, p).wait_send())
        if turn:
            c_copy(turn, z).wait_send()
    loop(1, count, lambda step: d_copy(step, mine).wait_send())

    def near_sends(step):
        n_copy(step, p).wait_send()
        k_copy(step, p).wait_send()

    loop(1, plane, near_sends)
    t_copy(core).wait_send()
    scan.settle()
    scan2.settle()


def whole(mid, cot, experts, weights, gate, up, down, weight, q, k, v, ld):
    count = lax.axis_size("sp")
    plane = count // GROUPS
    tokens, width = mid.shape
    cap = 4 * tokens // count
    slots = plane * cap
    gcap = slots // 2
    length, keys = q.shape
    heads = keys // DK
    values = v.shape[1]
    hide = gate.shape[1]
    share = width // count
    vrows = DV // count
    shape = jax.ShapeDtypeStruct
    dma = pltpu.SemaphoreType.DMA
    given = dict(
        mid=mid, cot=cot, ex=experts, wt=weights, q=q, k=k, v=v, ld=ld,
        gate=gate, up=up, down=down, weight=weight,
    )
    ins = {name + "_in": value for name, value in given.items()}
    outs = dict(
        gate_out=shape(gate.shape, BF16), up_out=shape(up.shape, BF16), down_out=shape(down.shape, BF16),
        out=shape((share, values), F32), dq=shape(q.shape, BF16), dk=shape(k.shape, BF16),
        dv=shape(v.shape, BF16), da=shape(q.shape, F32),
    )
    pieces = VMEM((count, vrows, keys), BF16)
    g3 = dma((2, GROUPS))
    scratch = {name: VMEM(value.shape, value.dtype) for name, value in given.items()}
    scratch |= dict(
        pick=VMEM((tokens, GROUPS * gcap), BF16),
        pack=VMEM((GROUPS, 2, gcap, width), BF16),
        pack_meta=VMEM((GROUPS, gcap, 128), F32),
        meta=VMEM((GROUPS, gcap, 128), F32),
        zbuf=VMEM((GROUPS, 2, gcap, width), BF16),
        wide=VMEM((GROUPS, 2, plane, cap, width), BF16),
        rows=VMEM((2, GROUPS, 2, plane, cap, width), BF16),
        hidden=VMEM((GROUPS, 2 * slots, hide), BF16),
        back_gate=VMEM((GROUPS, 2 * slots, hide), BF16),
        back_up=VMEM((GROUPS, 2 * slots, hide), BF16),
        part=VMEM((GROUPS, 2, slots, width), BF16),
        taken=VMEM((GROUPS, slots, width), BF16),
        result=VMEM((GROUPS, plane, cap, width), BF16),
        landed=VMEM((GROUPS, plane, cap, width), BF16),
        comb=VMEM((GROUPS, gcap, width), BF16),
        home=VMEM((GROUPS, gcap, width), BF16),
        rl=VMEM((length, keys), F32), dec_mine=VMEM((1, keys), F32), decs=VMEM((count, 1, keys), F32),
        total=VMEM((DV, keys), F32), score=VMEM((heads, length, length), F32),
        normed=VMEM((length, values), F32), normed_rows=VMEM((length, values), BF16),
        inv=VMEM((length, heads * 128), F32), near=VMEM((plane, length, values), BF16),
        piece=pieces, got=pieces, ready=pieces, inc=pieces,
        piece2=pieces, got2=pieces, ready2=pieces, fut=pieces,
        token=VMEM((tokens, width), BF16), both=VMEM((2, tokens, width), BF16),
        cut=VMEM((plane, length, GROUPS * share), BF16), tok=VMEM((plane, length, GROUPS * share), BF16),
        raw=VMEM((length, values), F32), run=VMEM((2, length, keys), F32),
        own=VMEM((GROUPS, share, values), F32), give=VMEM((GROUPS, share, values), BF16),
        take=VMEM((GROUPS, share, values), BF16),
        load_sem=dma((12,)), zs=g3, zr=g3, own_sem=g3, fs=g3, fr=g3,
        xs=dma((2, GROUPS, plane)), xr=dma((2, GROUPS, plane)),
        ps=dma((GROUPS,)), pr=dma((GROUPS,)), es=dma((GROUPS, plane)), er=dma((GROUPS, plane)),
        cs=dma((GROUPS,)), cr=dma((GROUPS,)), ds=dma((count,)), dr=dma((count,)),
        ns=dma((plane,)), nr=dma((plane,)), ks=dma((plane,)), kr=dma((plane,)), ts=dma, tr=dma,
        os=dma((GROUPS,)), orr=dma((GROUPS,)),
        s1=dma((count,)), r1=dma((count,)), s2=dma((count,)), r2=dma((count,)),
        s3=dma((count,)), r3=dma((count,)), s4=dma((count,)), r4=dma((count,)),
    )
    vmem = pl.BlockSpec(memory_space=VMEM)
    return pl.pallas_call(
        functools.partial(whole_kernel, tuple(ins) + tuple(outs) + tuple(scratch)),
        out_shape=list(outs.values()),
        in_specs=[pl.BlockSpec(memory_space=pltpu.HBM)] * len(ins),
        out_specs=[vmem] * len(outs),
        scratch_shapes=list(scratch.values()),
        compiler_params=pltpu.CompilerParams(
            collective_id=0, has_side_effects=True, vmem_limit_bytes=LIMIT
        ),
        name="whole",
    )(*[pltpu.with_memory_space_constraint(x, pltpu.HBM) for x in ins.values()])


LIMIT = 44 * 2**20


def emit_kernel(number, *refs):
    copies = [
        pltpu.make_async_copy(refs[n], refs[number + n], refs[2 * number].at[n]) for n in range(number)
    ]
    for copy in copies:
        copy.start()
    for copy in copies:
        copy.wait()


def emit(values):
    number = len(values)
    return pl.pallas_call(
        functools.partial(emit_kernel, number),
        out_shape=[jax.ShapeDtypeStruct(x.shape, x.dtype) for x in values],
        in_specs=[pl.BlockSpec(memory_space=VMEM)] * number,
        out_specs=[pl.BlockSpec(memory_space=pl.ANY)] * number,
        scratch_shapes=[pltpu.SemaphoreType.DMA((number,))],
        compiler_params=pltpu.CompilerParams(vmem_limit_bytes=12 * 2**20),
        name="emit",
    )(*values)


def body(
    mid_rows,
    cotangent,
    route_experts,
    route_weights,
    gate_weight,
    up_weight,
    down_weight,
    out_weight,
    queries,
    key_rows,
    value_rows,
    log_decay,
):
    results = whole(
        mid_rows, cotangent, route_experts.T, route_weights.T, gate_weight[0], up_weight[0], down_weight[0],
        out_weight, queries, key_rows, value_rows, log_decay,
    )
    gate_grad, up_grad, down_grad, out_grad, dq, dk, dv, da = emit(results)
    return (gate_grad[None], up_grad[None], down_grad[None], out_grad, dq, dk, dv, da)


def solution(mesh):
    in_specs = (
        P(("sp", "tp"), None),
        P(("sp", "tp"), None),
        P(("sp", "tp"), None),
        P(("sp", "tp"), None),
        P("sp", None, "tp"),
        P("sp", None, "tp"),
        P("sp", "tp", None),
        P(None, "tp"),
        P("sp", "tp"),
        P("sp", "tp"),
        P("sp", "tp"),
        P("sp", "tp"),
    )
    out_specs = (
        P("sp", None, "tp"),
        P("sp", None, "tp"),
        P("sp", "tp", None),
        P("sp", "tp"),
        P("sp", "tp"),
        P("sp", "tp"),
        P("sp", "tp"),
        P("sp", "tp"),
    )
    return jax.shard_map(body, mesh=mesh, in_specs=in_specs, out_specs=out_specs, check_vma=False)
```

time: 158 us -> 121 us (0.77)
  the two profiles are of different devices: /device:TPU:0 before, /device:TPU:11 now
where the time goes in v2:
time: 121 us
  Pallas kernels  120 us (99%)
    pallas_call x1, Pallas kernels, whole(): pl.pallas_call(functools.partial(whole_kernel, tuple(ins) + tuple(outs) +...  117 us
    pallas_call x1, Pallas kernels, emit(): pl.pallas_call(functools.partial(emit_kernel, number), out_shape=[jax.Sha...  3.1 us

profile of v2, /device:TPU:11, one launch (start us, length us, event | category | flops | bytes accessed | tf_op | source)
XLA Modules:
  0.0 120.8 jit_solution(5860793482159140451)
XLA Ops:
  0.6 117.1 %whole.1 = (bf16[2048,512]{1,0:T(8,128)(2,1)S(1)}, bf16[2048,512]{1,0:T(8,128)(2,1)S(1)}, bf16[512,2048]{1,0:T(8,128)(2,1)S(1)}, f32[128,1024]{1,0:T(8,128)S(1)}...) custom-call(bf16[64,2048]{1,0:T(8,128)(2,1)} %refs_0_.1, ...), custom_call_target="tpu_custom_call" | custom-call | tf_op jit(solution)/shard_map/whole/pallas_call | solution.py:665
  117.7 3.1 %emit.1 = (bf16[2048,512]{1,0:T(8,128)(2,1)}, bf16[2048,512]{1,0:T(8,128)(2,1)}, bf16[512,2048]{1,0:T(8,128)(2,1)}, f32[128,1024]{1,0:T(8,128)}, bf16[128,512]{1...) custom-call(bf16[2048,512]{1,0:T(8,128)(2,1)S(1)} %get-tuple-element.24.refs_0_, ...), custom_call_target="tpu_custom_call" | custom-call | tf_op jit(solution)/shard_map/emit/pallas_call | solution.py:693

commit v3 on v2

--- a/solution.py
+++ b/solution.py
@@ -74,13 +74,6 @@
 def greet_all():
     count, plane, mine, z, p, core = place()
     loop(1, count, lambda step: signal({"sp": lax.rem(mine + step, count)}))
-    signal({"tp": 1 - core})
-
-
-def greet_near():
-    count, plane, mine, z, p, core = place()
-    loop(1, plane, lambda step: signal({"sp": z * plane + lax.rem(p + step, plane)}))
-    loop(1, GROUPS, lambda step: signal({"sp": lax.rem(z + step, GROUPS) * plane + p}))
     signal({"tp": 1 - core})
 
 
@@ -125,59 +118,99 @@
 
 
 class Scan:
-    def __init__(self, total, got, ready, out, decs, s1, r1, s2, r2, backward):
-        self.refs = (total, got, ready, out, decs)
-        self.sems = (s1, r1, s2, r2)
+    def __init__(self, total, got, lift, zgot, ready, out, decs, zdecs, s1, r1, s2, r2, s3, r3, backward):
+        self.refs = (total, got, lift, zgot, ready, out, decs)
+        self.sems = (s1, r1, s2, r2, s3, r3)
         self.backward = backward
-
-    def first(self, step, there):
-        total, got, ready, out, decs = self.refs
+        self.zdecs = zdecs
+
+    def flat(self, last, step, there):
+        total, got, lift, zgot, ready, out, decs = self.refs
         count, plane, mine, z, p, core = place()
-        ahead = lax.rem(mine + step, count)
+        target = lax.rem(p + step, plane)
+        source, place_there = (ready, out) if last else (total, got)
+        sems = self.sems[4:] if last else self.sems[:2]
         return send(
-            total.at[ahead], got.at[there], self.sems[0].at[step], self.sems[1].at[step], {"sp": ahead}
-        )
-
-    def second(self, step, there):
-        total, got, ready, out, decs = self.refs
+            source.at[target], place_there.at[there], sems[0].at[step], sems[1].at[step],
+            {"sp": z * plane + target},
+        )
+
+    def rise(self, step):
+        total, got, lift, zgot, ready, out, decs = self.refs
         count, plane, mine, z, p, core = place()
-        ahead = lax.rem(mine + step, count)
-        return send(
-            ready.at[ahead], out.at[there], self.sems[2].at[step], self.sems[3].at[step], {"sp": ahead}
-        )
+        target = z - step if self.backward else z + step
+        ok = target >= 0 if self.backward else target < GROUPS
+        return (ok, send(lift, zgot.at[z], self.sems[2].at[step], self.sems[3].at[step], {"sp": target * plane + p}))
+
+    def fall(self, step):
+        total, got, lift, zgot, ready, out, decs = self.refs
+        count, plane, mine, z, p, core = place()
+        source = z + step if self.backward else z - step
+        ok = source < GROUPS if self.backward else source >= 0
+        return (ok, send(lift, zgot.at[source], self.sems[2].at[step], self.sems[3].at[step], {"sp": mine}))
+
+    def spot(self, position, size):
+        return size - 1 - position if self.backward else position
 
     def start(self):
-        total, got, ready, out, decs = self.refs
+        total, got, lift, zgot, ready, out, decs = self.refs
         count, plane, mine, z, p, core = place()
-        loop(1, count, lambda step: self.first(step, mine).start())
-        got[mine] = total[mine]
-
-    def middle(self):
-        total, got, ready, out, decs = self.refs
+        loop(1, plane, lambda step: self.flat(False, step, p).start())
+        got[p] = total[p]
+
+    def up(self):
+        total, got, lift, zgot, ready, out, decs = self.refs
         count, plane, mine, z, p, core = place()
-        loop(1, count, lambda step: self.first(step, lax.rem(mine + count - step, count)).wait_recv())
+        loop(1, plane, lambda step: self.flat(False, step, lax.rem(p + plane - step, plane)).wait_recv())
 
         def turn(position, carry):
-            index = count - 1 - position if self.backward else position
+            index = self.spot(position, plane)
+            return carry * decs[index] + got[index].astype(F32)
+
+        lift[...] = lax.fori_loop(0, plane, turn, jnp.zeros(lift.shape, F32)).astype(lift.dtype)
+        for step in range(1, GROUPS):
+            ok, copy = self.rise(step)
+            pl.when(ok)(copy.start)
+
+    def down(self):
+        total, got, lift, zgot, ready, out, decs = self.refs
+        count, plane, mine, z, p, core = place()
+        for step in range(1, GROUPS):
+            ok, copy = self.fall(step)
+            pl.when(ok)(copy.wait_recv)
+
+        def over(position, carry):
+            index = self.spot(position, GROUPS)
+            return carry * self.zdecs[index] + zgot[index].astype(F32)
+
+        carry = lax.fori_loop(
+            0, GROUPS - 1 - z if self.backward else z, over, jnp.zeros(lift.shape, F32)
+        )
+
+        def turn(position, carry):
+            index = self.spot(position, plane)
             ready[index] = carry.astype(ready.dtype)
             return carry * decs[index] + got[index].astype(F32)
 
-        lax.fori_loop(0, count, turn, jnp.zeros(got.shape[1:], F32))
-        loop(1, count, lambda step: self.second(step, mine).start())
-        out[mine] = ready[mine]
+        lax.fori_loop(0, plane, turn, carry)
+        loop(1, plane, lambda step: self.flat(True, step, p).start())
+        out[p] = ready[p]
 
     def finish(self):
         count, plane, mine, z, p, core = place()
-        loop(1, count, lambda step: self.second(step, lax.rem(mine + count - step, count)).wait_recv())
+        loop(1, plane, lambda step: self.flat(True, step, lax.rem(p + plane - step, plane)).wait_recv())
 
     def settle(self):
         count, plane, mine, z, p, core = place()
 
         def act(step):
-            self.first(step, mine).wait_send()
-            self.second(step, mine).wait_send()
-
-        loop(1, count, act)
+            self.flat(False, step, p).wait_send()
+            self.flat(True, step, p).wait_send()
+
+        loop(1, plane, act)
+        for step in range(1, GROUPS):
+            ok, copy = self.rise(step)
+            pl.when(ok)(copy.wait_send)
 
 
 STEPS = (0, 2, 1, 3)
@@ -247,23 +280,24 @@
     r.pack_meta[...] = packed_meta.reshape(r.pack_meta.shape)
     met(count)
 
-    def z_copy(step, there):
+    def z_copy(kind, step, there):
         target = lax.rem(z + step, GROUPS)
         return send(
-            r.pack.at[target], r.zbuf.at[there], r.zs.at[0, step], r.zr.at[0, step],
+            r.pack.at[target, kind], r.zbuf.at[there, kind], r.zs.at[kind, step], r.zr.at[kind, step],
             {"sp": target * plane + p},
         )
 
     def z_meta(step, there):
         target = lax.rem(z + step, GROUPS)
         return send(
-            r.pack_meta.at[target], r.meta.at[there], r.zs.at[1, step], r.zr.at[1, step],
+            r.pack_meta.at[target], r.meta.at[there], r.zs.at[2, step], r.zr.at[2, step],
             {"sp": target * plane + p},
         )
 
     for step in STEPS[1:]:
         z_meta(step, z).start()
-        z_copy(step, z).start()
+        for kind in range(2):
+            z_copy(kind, step, z).start()
     r.meta[z] = r.pack_meta[z]
     for name in LATER:
         loads[name].start()
@@ -280,28 +314,29 @@
             r.wide.at[turn, kind, p], r.rows.at[kind, turn, core, p], r.own_sem.at[kind, turn]
         )
 
-    def expand(turn, mid, cot):
+    def expand(kind, turn, ref):
         table = r.meta[source_of[turn]][:, :slots]
         chosen = (table > 0).astype(F32).astype(BF16)
-        ones = jnp.ones((gcap, 128), BF16)
-        t3 = split3(table)
-        scale = (mm(t3[0], ones, TN) + (mm(t3[1], ones, TN) + mm(t3[2], ones, TN)))[:, :1]
+        if kind:
+            ones = jnp.ones((gcap, 128), BF16)
+            t3 = split3(table)
+            scale = (mm(t3[0], ones, TN) + (mm(t3[1], ones, TN) + mm(t3[2], ones, TN)))[:, :1]
         chunk = 512
-        for kind, ref in enumerate((mid, cot)):
-            for n in range(0, width, chunk):
-                cols = slice(n, n + chunk)
-                value = mm(chosen, ref[:, cols], TN)
-                if kind:
-                    value = scale * value
-                r.wide[turn, kind, :, :, cols] = value.reshape(plane, cap, chunk).astype(BF16)
-            loop(1, plane, lambda step: x_copy(kind, turn, step, p).start())
-            own_copy(kind, turn).start()
+        for n in range(0, width, chunk):
+            cols = slice(n, n + chunk)
+            value = mm(chosen, ref[:, cols], TN)
+            if kind:
+                value = scale * value
+            r.wide[turn, kind, :, :, cols] = value.reshape(plane, cap, chunk).astype(BF16)
+        loop(1, plane, lambda step: x_copy(kind, turn, step, p).start())
+        own_copy(kind, turn).start()
 
     def receive(turn):
         step, source = STEPS[turn], source_of[turn]
         z_meta(step, source).wait_recv()
-        z_copy(step, source).wait_recv()
-        expand(turn, r.zbuf.at[source, 0], r.zbuf.at[source, 1])
+        for kind in range(2):
+            z_copy(kind, step, source).wait_recv()
+            expand(kind, turn, r.zbuf.at[source, kind])
 
     def forward(kind, turn, side):
         return send(
@@ -379,7 +414,8 @@
         else:
             r.home[z] = value
 
-    expand(0, r.pack.at[z, 0], r.pack.at[z, 1])
+    expand(0, 0, r.pack.at[z, 0])
+    expand(1, 0, r.pack.at[z, 1])
 
     for name in FIRST[4:]:
         loads[name].wait()
@@ -389,11 +425,15 @@
     r.dec_mine[...] = jnp.exp(r.rl[length - 1 :, :])
 
     def d_copy(step, there):
-        target = lax.rem(mine + step, count)
-        return send(r.dec_mine, r.decs.at[there], r.ds.at[step], r.dr.at[step], {"sp": target})
-
-    loop(1, count, lambda step: d_copy(step, mine).start())
-    r.decs[mine] = r.dec_mine[...]
+        target = lax.rem(p + step, plane)
+        return send(r.dec_mine, r.decs.at[there], r.ds.at[step], r.dr.at[step], {"sp": z * plane + target})
+
+    def w_copy(step, there):
+        target = lax.rem(z + step, GROUPS)
+        return send(r.dec_plane, r.zdecs.at[there], r.ws.at[step], r.wr.at[step], {"sp": target * plane + p})
+
+    loop(1, plane, lambda step: d_copy(step, p).start())
+    r.decs[p] = r.dec_mine[...]
 
     def head(h):
         return head_parts(r.rl[...], r.q, r.k, h, mid_row)
@@ -405,33 +445,40 @@
         total = mm2r(value, to_end, TN)
         r.total[:, h * DK : (h + 1) * DK] = total
         scatter_pieces(r.piece, total, h)
-    scan = Scan(r.piece, r.got, r.ready, r.inc, r.decs, r.s1, r.r1, r.s2, r.r2, False)
+    scan = Scan(r.piece, r.got, r.lift, r.zgot, r.ready, r.inc, r.decs, r.zdecs, r.s1, r.r1, r.s2, r.r2, r.s5, r.r5, False)
     scan.start()
 
     arrive(0)
-    receive(1)
+    loop(1, plane, lambda step: d_copy(step, lax.rem(p + plane - step, plane)).wait_recv())
+    r.dec_plane[...] = lax.fori_loop(0, plane, lambda n, x: x * r.decs[n], jnp.ones(r.dec_mine.shape, F32))
+    loop(1, GROUPS, lambda step: w_copy(step, z).start())
+    scan.up()
     for name in LATER[:3]:
         loads[name].wait()
     compute(0)
+    receive(1)
+    give_back(0)
     receive(2)
     arrive(1)
-    give_back(0)
+    receive(3)
     compute(1)
-    receive(3)
     arrive(2)
+    combine(0)
     give_back(1)
-    combine(0)
     compute(2)
-    loop(1, count, lambda step: d_copy(step, lax.rem(mine + count - step, count)).wait_recv())
-    scan.middle()
+    loop(1, GROUPS, lambda step: w_copy(step, lax.rem(z + GROUPS - step, GROUPS)).wait_recv())
+    scan.down()
     arrive(3)
     give_back(2)
+    compute(3)
     combine(1)
-    compute(3)
-    combine(2)
     give_back(3)
-
     scan.finish()
+
+    pair = z + 1 - 2 * lax.rem(z, 2)
+    across = lax.rem(z + 2, GROUPS)
+
+    far = lax.rem(pair + 2, GROUPS)
 
     def n_copy(step, there):
         target = lax.rem(p + step, plane)
@@ -452,10 +499,9 @@
         r.normed[:, wide] = out
         r.normed_rows[:, wide] = out.astype(BF16)
         r.inv[:, h * 128 : (h + 1) * 128] = jnp.broadcast_to(inverse, (length, 128))
+    loop(1, plane, lambda step: n_copy(step, p).start())
     r.near[p] = r.normed_rows[...]
-    loop(1, plane, lambda step: n_copy(step, p).start())
-
-    combine(3)
+    combine(2)
     all_rows = GROUPS * 2 * slots
 
     def gates(n):
@@ -465,6 +511,14 @@
         r.up_out[cols, :] = mm(rows, r.back_up[...].reshape(all_rows, hide), TN).astype(BF16)
 
     loop(0, width // 256, gates)
+    combine(3)
+
+    def downs(n):
+        cols = pl.ds(pl.multiple_of(n * 256, 256), 256)
+        hidden = r.hidden[:, :, cols].reshape(all_rows, 256)
+        r.down_out[cols, :] = mm(hidden, r.rows[1].reshape(all_rows, width), TN).astype(BF16)
+
+    loop(0, hide // 256, downs)
 
     for turn in range(1, GROUPS):
         c_copy(turn, lax.rem(z + STEPS[turn], GROUPS)).wait_recv()
@@ -472,28 +526,32 @@
         r.cot[...].astype(F32) + mm(r.pick[...], r.home[...].reshape(GROUPS * gcap, width))
     ).astype(BF16)
     r.token[...] = token
-    r.both[core] = token
-
-    def t_copy(side):
-        return send(r.token, r.both.at[side], r.ts, r.tr, {"tp": 1 - core})
-
-    t_copy(core).start()
-    t_copy(1 - core).wait_recv()
-
     for other in range(plane):
         for g in range(GROUPS):
             start = (g * plane + other) * share
-            for side in range(2):
-                r.cut[other, side * tokens : (side + 1) * tokens, g * share : (g + 1) * share] = r.both[
-                    side, :, start : start + share
-                ]
+            r.cut[other, g] = token[:, start : start + share]
+    r.both[core] = token
+
+    def t_copy(side):
+        return send(r.token, r.both.at[side], r.ts, r.tr, {"tp": 1 - core})
 
     def k_copy(step, there):
         target = lax.rem(p + step, plane)
-        return send(r.cut.at[target], r.tok.at[there], r.ks.at[step], r.kr.at[step], {"sp": z * plane + target})
-
+        return send(
+            r.cut.at[target], r.tok.at[there, core], r.ks.at[step], r.kr.at[step], {"sp": z * plane + target}
+        )
+
+    def k_pass(step, side):
+        there = lax.rem(p + plane - step, plane)
+        return send(
+            r.tok.at[there, side], r.tok.at[there, side], r.js.at[step], r.jr.at[step], {"tp": 1 - core}
+        )
+
+    t_copy(core).start()
     loop(1, plane, lambda step: k_copy(step, p).start())
-    r.tok[p] = r.cut[p]
+    r.tok[p, core] = r.cut[p]
+    k_pass(0, core).start()
+    t_copy(1 - core).wait_recv()
 
     loads["weight"].wait()
     for h in range(heads):
@@ -506,14 +564,16 @@
         r.raw[:, wide] = value
         rl_h, mid, last, qs, kf = head(h)
         scatter_pieces(r.piece2, mm3(split2(value), split2(qs * jnp.exp(rl_h)), TN), h)
-    scan2 = Scan(r.piece2, r.got2, r.ready2, r.fut, r.decs, r.s3, r.r3, r.s4, r.r4, True)
+    scan2 = Scan(r.piece2, r.got2, r.lift2, r.zgot2, r.ready2, r.fut, r.decs, r.zdecs, r.s3, r.r3, r.s4, r.r4, r.s6, r.r6, True)
     scan2.start()
 
-    def o_copy(step, there):
-        target = lax.rem(z + step, GROUPS)
-        return send(
-            r.give.at[target], r.take.at[there], r.os.at[step], r.orr.at[step], {"sp": target * plane + p}
-        )
+    def o_copy(n):
+        aim = across if n == 2 else pair
+        return send(r.give.at[n], r.take.at[n], r.os.at[n], r.orr.at[n], {"sp": aim * plane + p})
+
+    def terms(g):
+        rows = plane * length
+        return mm(r.tok[:, :, g].reshape(rows, share), r.near[...].reshape(rows, r.near.shape[2]), TN)
 
     for h in range(heads):
         rl_h, mid, last, qs, kf = head(h)
@@ -529,25 +589,23 @@
         r.run[1, :, cols] = qs * dq
         r.raw[:, wide] = mm3(split2(r.score[h]), back, TN)
 
-    loop(1, plane, lambda step: k_copy(step, lax.rem(p + plane - step, plane)).wait_recv())
+    def k_arrive(step):
+        k_copy(step, lax.rem(p + plane - step, plane)).wait_recv()
+        k_pass(step, core).start()
+
+    loop(1, plane, k_arrive)
+    scan2.up()
+    loop(0, plane, lambda step: k_pass(step, 1 - core).wait_recv())
     loop(1, plane, lambda step: n_copy(step, lax.rem(p + plane - step, plane)).wait_recv())
-    near = r.near[...].reshape(plane * length, r.near.shape[2])
-    for g in range(GROUPS):
-        value = mm(r.tok[:, :, g * share : (g + 1) * share].reshape(plane * length, share), near, TN)
-        r.own[g] = value
-        r.give[g] = value.astype(BF16)
-    o_copy(1, z).start()
-    scan2.middle()
-    o_copy(2, z).start()
-    o_copy(3, z).start()
-
-    def downs(n):
-        cols = pl.ds(pl.multiple_of(n * 256, 256), 256)
-        hidden = r.hidden[:, :, cols].reshape(all_rows, 256)
-        r.down_out[cols, :] = mm(hidden, r.rows[1].reshape(all_rows, width), TN).astype(BF16)
-
-    loop(0, hide // 256, downs)
-
+    for n, g in enumerate((far, pair)):
+        r.give[n] = terms(g).astype(BF16)
+        o_copy(n).start()
+    r.own[1] = terms(across)
+    r.own[0] = terms(z)
+    o_copy(0).wait_recv()
+    r.give[2] = (r.own[1] + r.take[0].astype(F32)).astype(BF16)
+    o_copy(2).start()
+    scan2.down()
     scan2.finish()
     high_b = tri(length, False).astype(F32).astype(BF16)
     for h in range(heads):
@@ -565,17 +623,16 @@
         end = jnp.exp(last) * state + r.total[:, cols]
         r.da[:, cols] = later + jnp.sum(end * future.astype(F32), axis=0, keepdims=True)
 
-    for step in STEPS[1:]:
-        o_copy(step, lax.rem(z + GROUPS - step, GROUPS)).wait_recv()
-    sides = [lax.rem(z + step, GROUPS) for step in (1, 2, 3)]
-    r.out[...] = (r.own[z] + r.take[sides[0]].astype(F32)) + (
-        r.take[sides[1]].astype(F32) + r.take[sides[2]].astype(F32)
-    )
-
+    o_copy(1).wait_recv()
+    o_copy(2).wait_recv()
+    r.out[...] = r.own[0] + (r.take[1].astype(F32) + r.take[2].astype(F32))
+
+    for n in range(3):
+        o_copy(n).wait_send()
     for step in STEPS[1:]:
         z_meta(step, z).wait_send()
-        z_copy(step, z).wait_send()
-        o_copy(step, z).wait_send()
+        for kind in range(2):
+            z_copy(kind, step, z).wait_send()
     for turn in range(GROUPS):
         for kind in range(2):
             loop(1, plane, lambda step: x_copy(kind, turn, step, p).wait_send())
@@ -584,13 +641,12 @@
         loop(1, plane, lambda step: e_copy(turn, step, p).wait_send())
         if turn:
             c_copy(turn, z).wait_send()
-    loop(1, count, lambda step: d_copy(step, mine).wait_send())
-
-    def near_sends(step):
-        n_copy(step, p).wait_send()
-        k_copy(step, p).wait_send()
-
-    loop(1, plane, near_sends)
+    loop(1, plane, lambda step: d_copy(step, p).wait_send())
+    loop(1, GROUPS, lambda step: w_copy(step, z).wait_send())
+
+    loop(1, plane, lambda step: n_copy(step, p).wait_send())
+    loop(1, plane, lambda step: k_copy(step, p).wait_send())
+    loop(0, plane, lambda step: k_pass(step, core).wait_send())
     t_copy(core).wait_send()
     scan.settle()
     scan2.settle()
@@ -608,7 +664,6 @@
     values = v.shape[1]
     hide = gate.shape[1]
     share = width // count
-    vrows = DV // count
     shape = jax.ShapeDtypeStruct
     dma = pltpu.SemaphoreType.DMA
     given = dict(
@@ -621,7 +676,9 @@
         out=shape((share, values), F32), dq=shape(q.shape, BF16), dk=shape(k.shape, BF16),
         dv=shape(v.shape, BF16), da=shape(q.shape, F32),
     )
-    pieces = VMEM((count, vrows, keys), BF16)
+    pieces = VMEM((plane, DV // plane, keys), BF16)
+    lifts = VMEM((DV // plane, keys), BF16)
+    zgots = VMEM((GROUPS, DV // plane, keys), BF16)
     g3 = dma((2, GROUPS))
     scratch = {name: VMEM(value.shape, value.dtype) for name, value in given.items()}
     scratch |= dict(
@@ -641,25 +698,26 @@
         landed=VMEM((GROUPS, plane, cap, width), BF16),
         comb=VMEM((GROUPS, gcap, width), BF16),
         home=VMEM((GROUPS, gcap, width), BF16),
-        rl=VMEM((length, keys), F32), dec_mine=VMEM((1, keys), F32), decs=VMEM((count, 1, keys), F32),
+        rl=VMEM((length, keys), F32), dec_mine=VMEM((1, keys), F32), decs=VMEM((plane, 1, keys), F32), dec_plane=VMEM((1, keys), F32),
+        zdecs=VMEM((GROUPS, 1, keys), F32),
         total=VMEM((DV, keys), F32), score=VMEM((heads, length, length), F32),
         normed=VMEM((length, values), F32), normed_rows=VMEM((length, values), BF16),
         inv=VMEM((length, heads * 128), F32), near=VMEM((plane, length, values), BF16),
-        piece=pieces, got=pieces, ready=pieces, inc=pieces,
+        piece=pieces, got=pieces, ready=pieces, inc=pieces, lift=lifts, zgot=zgots, lift2=lifts, zgot2=zgots,
         piece2=pieces, got2=pieces, ready2=pieces, fut=pieces,
         token=VMEM((tokens, width), BF16), both=VMEM((2, tokens, width), BF16),
-        cut=VMEM((plane, length, GROUPS * share), BF16), tok=VMEM((plane, length, GROUPS * share), BF16),
+        cut=VMEM((plane, GROUPS, tokens, share), BF16), tok=VMEM((plane, 2, GROUPS, tokens, share), BF16),
         raw=VMEM((length, values), F32), run=VMEM((2, length, keys), F32),
-        own=VMEM((GROUPS, share, values), F32), give=VMEM((GROUPS, share, values), BF16),
-        take=VMEM((GROUPS, share, values), BF16),
-        load_sem=dma((12,)), zs=g3, zr=g3, own_sem=g3, fs=g3, fr=g3,
+        own=VMEM((2, share, values), F32), give=VMEM((3, share, values), BF16), take=VMEM((3, share, values), BF16),
+        load_sem=dma((12,)), zs=dma((3, GROUPS)), zr=dma((3, GROUPS)), own_sem=g3, fs=g3, fr=g3,
         xs=dma((2, GROUPS, plane)), xr=dma((2, GROUPS, plane)),
         ps=dma((GROUPS,)), pr=dma((GROUPS,)), es=dma((GROUPS, plane)), er=dma((GROUPS, plane)),
-        cs=dma((GROUPS,)), cr=dma((GROUPS,)), ds=dma((count,)), dr=dma((count,)),
-        ns=dma((plane,)), nr=dma((plane,)), ks=dma((plane,)), kr=dma((plane,)), ts=dma, tr=dma,
-        os=dma((GROUPS,)), orr=dma((GROUPS,)),
-        s1=dma((count,)), r1=dma((count,)), s2=dma((count,)), r2=dma((count,)),
-        s3=dma((count,)), r3=dma((count,)), s4=dma((count,)), r4=dma((count,)),
+        cs=dma((GROUPS,)), cr=dma((GROUPS,)), ds=dma((plane,)), dr=dma((plane,)),
+        ws=dma((GROUPS,)), wr=dma((GROUPS,)),
+        ns=dma((plane,)), nr=dma((plane,)), ks=dma((plane,)), kr=dma((plane,)), js=dma((plane,)), jr=dma((plane,)),
+        ts=dma, tr=dma, os=dma((3,)), orr=dma((3,)),
+        s1=dma((plane,)), r1=dma((plane,)), s2=dma((GROUPS,)), r2=dma((GROUPS,)), s5=dma((plane,)), r5=dma((plane,)),
+        s3=dma((plane,)), r3=dma((plane,)), s4=dma((GROUPS,)), r4=dma((GROUPS,)), s6=dma((plane,)), r6=dma((plane,)),
     )
     vmem = pl.BlockSpec(memory_space=VMEM)
     return pl.pallas_call(

time: 121 us -> 107 us (0.88)
  the two profiles are of different devices: /device:TPU:11 before, /device:TPU:0 now
where the time goes in v3:
time: 107 us; the launch traced here: 106 us
  Pallas kernels  106 us (99%)
    pallas_call x1, Pallas kernels, whole(): pl.pallas_call(functools.partial(whole_kernel, tuple(ins) + tuple(outs) +...  103 us
    pallas_call x1, Pallas kernels, emit(): pl.pallas_call(functools.partial(emit_kernel, number), out_shape=[jax.Sha...  3.1 us

profile of v3, /device:TPU:0, one launch (start us, length us, event | category | flops | bytes accessed | tf_op | source)
XLA Modules:
  0.0 106.4 jit_solution(17403945492797917555)
XLA Ops:
  0.6 102.7 %whole.1 = (bf16[2048,512]{1,0:T(8,128)(2,1)S(1)}, bf16[2048,512]{1,0:T(8,128)(2,1)S(1)}, bf16[512,2048]{1,0:T(8,128)(2,1)S(1)}, f32[128,1024]{1,0:T(8,128)S(1)}...) custom-call(bf16[64,2048]{1,0:T(8,128)(2,1)} %refs_0_.1, ...), custom_call_target="tpu_custom_call" | custom-call | tf_op jit(solution)/shard_map/whole/pallas_call | solution.py:723
  103.3 3.1 %emit.1 = (bf16[2048,512]{1,0:T(8,128)(2,1)}, bf16[2048,512]{1,0:T(8,128)(2,1)}, bf16[512,2048]{1,0:T(8,128)(2,1)}, f32[128,1024]{1,0:T(8,128)}, bf16[128,512]{1...) custom-call(bf16[2048,512]{1,0:T(8,128)(2,1)S(1)} %get-tuple-element.24.refs_0_, ...), custom_call_target="tpu_custom_call" | custom-call | tf_op jit(solution)/shard_map/emit/pallas_call | solution.py:751

commit v4 on v3

--- a/solution.py
+++ b/solution.py
@@ -213,7 +213,7 @@
             pl.when(ok)(copy.wait_send)
 
 
-STEPS = (0, 2, 1, 3)
+STEPS = (0, 3, 2, 1)
 FIRST = ("ex", "wt", "mid", "cot", "ld", "q", "k", "v")
 LATER = ("gate", "up", "down", "weight")
 
@@ -274,10 +274,12 @@
     rank1 = jnp.sum(jnp.where(hit1, before, 0.0), axis=1, keepdims=True)
     slot0 = (e0 - group * plane) * cap + rank0
     slot1 = (e1 - group * plane) * cap + rank1
-    weights = jnp.where(slot0 == lane_f, w0, 0.0) + jnp.where(slot1 == lane_f, w1, 0.0)
-    w3 = split3(weights)
-    packed_meta = mm(pick, w3[0], TN) + (mm(pick, w3[1], TN) + mm(pick, w3[2], TN))
-    r.pack_meta[...] = packed_meta.reshape(r.pack_meta.shape)
+    item = lax.broadcasted_iota(jnp.int32, (tokens, 8), 1)
+    facts = jnp.where(item == 0, slot0, 0.0) + jnp.where(item == 1, slot1, 0.0)
+    facts = split3(facts + jnp.where(item == 2, w0, 0.0) + jnp.where(item == 3, w1, 0.0))
+    for g in range(GROUPS):
+        some = ((group == g) & (rank_group == lane_f)).astype(F32).astype(BF16)
+        r.pack_meta[g] = mm(facts[0], some, TN) + (mm(facts[1], some, TN) + mm(facts[2], some, TN))
     met(count)
 
     def z_copy(kind, step, there):
@@ -314,17 +316,20 @@
             r.wide.at[turn, kind, p], r.rows.at[kind, turn, core, p], r.own_sem.at[kind, turn]
         )
 
+    def slot_table(turn):
+        known = r.meta[source_of[turn]][:, :gcap]
+        slot = lax.broadcasted_iota(jnp.int32, (slots, gcap), 0).astype(F32)
+        return jnp.where(known[0:1] == slot, known[2:3], 0.0) + jnp.where(known[1:2] == slot, known[3:4], 0.0)
+
     def expand(kind, turn, ref):
-        table = r.meta[source_of[turn]][:, :slots]
+        table = slot_table(turn)
         chosen = (table > 0).astype(F32).astype(BF16)
         if kind:
-            ones = jnp.ones((gcap, 128), BF16)
-            t3 = split3(table)
-            scale = (mm(t3[0], ones, TN) + (mm(t3[1], ones, TN) + mm(t3[2], ones, TN)))[:, :1]
+            scale = jnp.sum(table, axis=1, keepdims=True)
         chunk = 512
         for n in range(0, width, chunk):
             cols = slice(n, n + chunk)
-            value = mm(chosen, ref[:, cols], TN)
+            value = mm(chosen, ref[:, cols])
             if kind:
                 value = scale * value
             r.wide[turn, kind, :, :, cols] = value.reshape(plane, cap, chunk).astype(BF16)
@@ -405,9 +410,8 @@
 
     def combine(turn):
         loop(1, plane, lambda step: e_copy(turn, step, lax.rem(p + plane - step, plane)).wait_recv())
-        table = r.meta[source_of[turn]][:, :slots]
-        chosen = (table > 0).astype(F32).astype(BF16)
-        value = mm(chosen, r.landed[turn].reshape(slots, width)).astype(BF16)
+        chosen = (slot_table(turn) > 0).astype(F32).astype(BF16)
+        value = mm(chosen, r.landed[turn].reshape(slots, width), TN).astype(BF16)
         if turn:
             r.comb[turn] = value
             c_copy(turn, z).start()
@@ -493,7 +497,7 @@
         r.score[h] = score
         decayed = split2(qs * jnp.exp(rl_h))
         state = r.inc[:, :, h * DK : (h + 1) * DK].reshape(DV, DK)
-        raw = mm2l(split2(score), r.v[:, wide]) + mm2l(decayed, state, NT)
+        raw = mm2l(split2(score), r.v[:, wide]) + mm3(decayed, split2(state), NT)
         inverse = lax.rsqrt(jnp.mean(raw * raw, axis=1, keepdims=True) + epsilon)
         out = raw * inverse
         r.normed[:, wide] = out
@@ -567,9 +571,13 @@
     scan2 = Scan(r.piece2, r.got2, r.lift2, r.zgot2, r.ready2, r.fut, r.decs, r.zdecs, r.s3, r.r3, r.s4, r.r4, r.s6, r.r6, True)
     scan2.start()
 
-    def o_copy(n):
+    half_cols = r.give.shape[3]
+
+    def o_copy(n, part):
         aim = across if n == 2 else pair
-        return send(r.give.at[n], r.take.at[n], r.os.at[n], r.orr.at[n], {"sp": aim * plane + p})
+        return send(
+            r.give.at[n, part], r.take.at[n, part], r.os.at[n, part], r.orr.at[n, part], {"sp": aim * plane + p}
+        )
 
     def terms(g):
         rows = plane * length
@@ -583,7 +591,7 @@
         dots = split2(jnp.where(low, mm2l(back, r.v[:, wide], NT), 0.0))
         up_scale, down_scale = jnp.exp(rl_h - mid), jnp.exp(mid - rl_h)
         state = r.inc[:, :, cols].reshape(DV, DK)
-        dq = up_scale * mm3(dots, split2(kf * down_scale)) + jnp.exp(rl_h) * mm2l(back, state)
+        dq = up_scale * mm3(dots, split2(kf * down_scale)) + jnp.exp(rl_h) * mm3(back, split2(state))
         r.dq[:, cols] = (dq * DK ** (-0.5)).astype(BF16)
         r.run[0, :, cols] = down_scale * mm3(dots, split2(qs * up_scale), TN)
         r.run[1, :, cols] = qs * dq
@@ -598,13 +606,17 @@
     loop(0, plane, lambda step: k_pass(step, 1 - core).wait_recv())
     loop(1, plane, lambda step: n_copy(step, lax.rem(p + plane - step, plane)).wait_recv())
     for n, g in enumerate((far, pair)):
-        r.give[n] = terms(g).astype(BF16)
-        o_copy(n).start()
+        value = terms(g).astype(BF16)
+        for part in range(2):
+            r.give[n, part] = value[:, part * half_cols : (part + 1) * half_cols]
+            o_copy(n, part).start()
     r.own[1] = terms(across)
     r.own[0] = terms(z)
-    o_copy(0).wait_recv()
-    r.give[2] = (r.own[1] + r.take[0].astype(F32)).astype(BF16)
-    o_copy(2).start()
+    for part in range(2):
+        o_copy(0, part).wait_recv()
+        cols = slice(part * half_cols, (part + 1) * half_cols)
+        r.give[2, part] = (r.own[1, :, cols] + r.take[0, part].astype(F32)).astype(BF16)
+        o_copy(2, part).start()
     scan2.down()
     scan2.finish()
     high_b = tri(length, False).astype(F32).astype(BF16)
@@ -614,21 +626,24 @@
         wide = slice(h * DV, (h + 1) * DV)
         future = r.fut[:, :, cols].reshape(DV, DK)
         to_end = jnp.exp(last - rl_h)
-        dk = r.run[0, :, cols] + to_end * mm(r.v[:, wide], future)
+        dk = r.run[0, :, cols] + to_end * mm2r(r.v[:, wide], split2(future))
         r.dk[:, cols] = dk.astype(BF16)
-        r.dv[:, wide] = (r.raw[:, wide] + mm2l(split2(kf * to_end), future, NT)).astype(BF16)
+        r.dv[:, wide] = (r.raw[:, wide] + mm3(split2(kf * to_end), split2(future), NT)).astype(BF16)
         change = split3(r.run[1, :, cols] - kf * dk)
         later = mm(high_b, change[0]) + (mm(high_b, change[1]) + mm(high_b, change[2]))
         state = r.inc[:, :, cols].reshape(DV, DK).astype(F32)
         end = jnp.exp(last) * state + r.total[:, cols]
         r.da[:, cols] = later + jnp.sum(end * future.astype(F32), axis=0, keepdims=True)
 
-    o_copy(1).wait_recv()
-    o_copy(2).wait_recv()
-    r.out[...] = r.own[0] + (r.take[1].astype(F32) + r.take[2].astype(F32))
+    for part in range(2):
+        o_copy(1, part).wait_recv()
+        o_copy(2, part).wait_recv()
+        cols = slice(part * half_cols, (part + 1) * half_cols)
+        r.out[:, cols] = r.own[0, :, cols] + (r.take[1, part].astype(F32) + r.take[2, part].astype(F32))
 
     for n in range(3):
-        o_copy(n).wait_send()
+        for part in range(2):
+            o_copy(n, part).wait_send()
     for step in STEPS[1:]:
         z_meta(step, z).wait_send()
         for kind in range(2):
@@ -676,16 +691,16 @@
         out=shape((share, values), F32), dq=shape(q.shape, BF16), dk=shape(k.shape, BF16),
         dv=shape(v.shape, BF16), da=shape(q.shape, F32),
     )
-    pieces = VMEM((plane, DV // plane, keys), BF16)
-    lifts = VMEM((DV // plane, keys), BF16)
-    zgots = VMEM((GROUPS, DV // plane, keys), BF16)
+    pieces = VMEM((plane, DV // plane, keys), F32)
+    lifts = VMEM((DV // plane, keys), F32)
+    zgots = VMEM((GROUPS, DV // plane, keys), F32)
     g3 = dma((2, GROUPS))
     scratch = {name: VMEM(value.shape, value.dtype) for name, value in given.items()}
     scratch |= dict(
         pick=VMEM((tokens, GROUPS * gcap), BF16),
         pack=VMEM((GROUPS, 2, gcap, width), BF16),
-        pack_meta=VMEM((GROUPS, gcap, 128), F32),
-        meta=VMEM((GROUPS, gcap, 128), F32),
+        pack_meta=VMEM((GROUPS, 8, 128), F32),
+        meta=VMEM((GROUPS, 8, 128), F32),
         zbuf=VMEM((GROUPS, 2, gcap, width), BF16),
         wide=VMEM((GROUPS, 2, plane, cap, width), BF16),
         rows=VMEM((2, GROUPS, 2, plane, cap, width), BF16),
@@ -708,14 +723,15 @@
         token=VMEM((tokens, width), BF16), both=VMEM((2, tokens, width), BF16),
         cut=VMEM((plane, GROUPS, tokens, share), BF16), tok=VMEM((plane, 2, GROUPS, tokens, share), BF16),
         raw=VMEM((length, values), F32), run=VMEM((2, length, keys), F32),
-        own=VMEM((2, share, values), F32), give=VMEM((3, share, values), BF16), take=VMEM((3, share, values), BF16),
+        own=VMEM((2, share, values), F32), give=VMEM((3, 2, share, values // 2), BF16),
+        take=VMEM((3, 2, share, values // 2), BF16),
         load_sem=dma((12,)), zs=dma((3, GROUPS)), zr=dma((3, GROUPS)), own_sem=g3, fs=g3, fr=g3,
         xs=dma((2, GROUPS, plane)), xr=dma((2, GROUPS, plane)),
         ps=dma((GROUPS,)), pr=dma((GROUPS,)), es=dma((GROUPS, plane)), er=dma((GROUPS, plane)),
         cs=dma((GROUPS,)), cr=dma((GROUPS,)), ds=dma((plane,)), dr=dma((plane,)),
         ws=dma((GROUPS,)), wr=dma((GROUPS,)),
         ns=dma((plane,)), nr=dma((plane,)), ks=dma((plane,)), kr=dma((plane,)), js=dma((plane,)), jr=dma((plane,)),
-        ts=dma, tr=dma, os=dma((3,)), orr=dma((3,)),
+        ts=dma, tr=dma, os=dma((3, 2)), orr=dma((3, 2)),
         s1=dma((plane,)), r1=dma((plane,)), s2=dma((GROUPS,)), r2=dma((GROUPS,)), s5=dma((plane,)), r5=dma((plane,)),
         s3=dma((plane,)), r3=dma((plane,)), s4=dma((GROUPS,)), r4=dma((GROUPS,)), s6=dma((plane,)), r6=dma((plane,)),
     )

time: 107 us -> 115 us (1.075)
  Pallas kernels: 106 us -> 114 us
    pallas_call x1, Pallas kernels: 103 us -> 111 us  [whole(): pl.pallas_call(functools.partial(whole_kernel, tuple(ins) + tuple(outs) +...]
where the time goes in v4:
time: 115 us
  Pallas kernels  114 us (99%)
    pallas_call x1, Pallas kernels, whole(): pl.pallas_call(functools.partial(whole_kernel, tuple(ins) + tuple(outs) +...  111 us
    pallas_call x1, Pallas kernels, emit(): pl.pallas_call(functools.partial(emit_kernel, number), out_shape=[jax.Sha...  3.1 us

profile of v4, /device:TPU:0, one launch (start us, length us, event | category | flops | bytes accessed | tf_op | source)
XLA Modules:
  0.0 114.5 jit_solution(9439507387464869034)
XLA Ops:
  0.6 110.8 %whole.1 = (bf16[2048,512]{1,0:T(8,128)(2,1)S(1)}, bf16[2048,512]{1,0:T(8,128)(2,1)S(1)}, bf16[512,2048]{1,0:T(8,128)(2,1)S(1)}, f32[128,1024]{1,0:T(8,128)S(1)}...) custom-call(bf16[64,2048]{1,0:T(8,128)(2,1)} %refs_0_.1, ...), custom_call_target="tpu_custom_call" | custom-call | tf_op jit(solution)/shard_map/whole/pallas_call | solution.py:739
  111.4 3.1 %emit.1 = (bf16[2048,512]{1,0:T(8,128)(2,1)}, bf16[2048,512]{1,0:T(8,128)(2,1)}, bf16[512,2048]{1,0:T(8,128)(2,1)}, f32[128,1024]{1,0:T(8,128)}, bf16[128,512]{1...) custom-call(bf16[2048,512]{1,0:T(8,128)(2,1)S(1)} %get-tuple-element.24.refs_0_, ...), custom_call_target="tpu_custom_call" | custom-call | tf_op jit(solution)/shard_map/emit/pallas_call | solution.py:767
